TPU v7x, 32 devices: a whole 2x2x4 slice. The times are simulated.
32 devices in a mesh: gr: 2 (over y), fs: 8 (over z, core), tp: 2 (over x).
Axes of the slice: x: 2, y: 2, z: 4, core: 2. Of those that a mesh axis runs over, the one named last changes fastest.
Arguments:
- prompt: bfloat16 [2048, 2048], P(('gr', 'fs')), may hold values from -6 to 6
- expert_ids: int32 [2048, 2], P(('gr', 'fs')), may hold values from 0 to 7, all different within a row; in each aligned block of 128 rows (0 to 127, 128 to 255, ...) at most 32 rows name the same one
- route_weights: float32 [2048, 2], P(('gr', 'fs')), may hold values from 0.2 to 1
- gate_master: float32 [8, 2048, 8192], P('gr', 'fs', 'tp'), may hold values from -0.125 to 0.125
- up_master: float32 [8, 2048, 8192], P('gr', 'fs', 'tp'), may hold values from -0.125 to 0.125
- down_master: float32 [8, 8192, 2048], P('gr', 'fs', 'tp'), may hold values from -0.0625 to 0.0625
- ffn_gain: float32 [2048], P('fs'), may hold values from 0.1 to 1.9
Outputs:
- gate_serving: bfloat16 [8, 2048, 8192], P('tp', None, 'fs')
- up_serving: bfloat16 [8, 2048, 8192], P('tp', None, 'fs')
- down_serving: bfloat16 [8, 8192, 2048], P('tp', 'fs')
- mixed: bfloat16 [2048, 2048], P(('gr', 'fs', 'tp'))
Inputs may be any that keep to these rules, and one draw needn't show every extreme that they name: `expert_ids`: the two experts of a token differ; the rows of one index of gr and fs name each expert exactly 32 times.
All inputs are finite; a program needn't handle non-finite values.
Results may differ from a plain program's by a relative error of at most 0.025.
Values may be sent and summed in bfloat16 or wider, within the bound.
No kernel may reach another device: no remote copies, remote signals or barrier semaphores. Data moves between devices by JAX's collectives and lax.ppermute only.
A program may use at most 256 MiB of HBM per device.

v0:
```python
import jax
import jax.numpy as jnp
from jax import lax
from jax.sharding import PartitionSpec as P

EXPERTS = 8
SLOTS = 32


NORM_EPS = 1e-06


def regroup_rows(weights, group_count, shard_count):
    local_experts, row_total, width = weights.shape
    stacked = weights.reshape(
        local_experts, group_count, shard_count, row_total // (group_count * shard_count), width
    )
    return stacked.transpose(0, 2, 1, 3, 4).reshape(local_experts, row_total, width)


def body(prompt, expert_ids, route_weights, gate_master, up_master, down_master, ffn_gain):
    group_count = lax.axis_size("gr")
    shard_count = lax.axis_size("fs")
    folding = ffn_gain[None, :, None]
    gate_local = (gate_master * folding).astype(jnp.bfloat16)
    up_local = (up_master * folding).astype(jnp.bfloat16)
    down_local = down_master.astype(jnp.bfloat16)
    gate_rows, up_rows = (
        lax.all_to_all(gate_local, "gr", split_axis=1, concat_axis=0, tiled=True),
        lax.all_to_all(up_local, "gr", split_axis=1, concat_axis=0, tiled=True),
    )
    down_whole = lax.all_gather(down_local, "gr", axis=0, tiled=True)
    gate_cols, up_cols = (
        lax.all_to_all(
            lax.all_to_all(gate_rows, "tp", split_axis=0, concat_axis=2, tiled=True),
            "fs",
            split_axis=2,
            concat_axis=1,
            tiled=True,
        ),
        lax.all_to_all(
            lax.all_to_all(up_rows, "tp", split_axis=0, concat_axis=2, tiled=True),
            "fs",
            split_axis=2,
            concat_axis=1,
            tiled=True,
        ),
    )
    down_serving = lax.all_to_all(down_whole, "tp", split_axis=0, concat_axis=2, tiled=True)
    gate_joined, up_joined = (
        lax.all_gather(gate_cols, "gr", axis=1, tiled=True),
        lax.all_gather(up_cols, "gr", axis=1, tiled=True),
    )
    gate_serving = regroup_rows(gate_joined, group_count, shard_count)
    up_serving = regroup_rows(up_joined, group_count, shard_count)
    token_count = prompt.shape[0]
    local_experts = gate_serving.shape[0]
    xfloat = prompt.astype(jnp.float32)
    normed = (
        xfloat * lax.rsqrt(jnp.mean(xfloat * xfloat, axis=1, keepdims=True) + NORM_EPS)
    ).astype(jnp.bfloat16)
    first_expert = lax.axis_index("tp") * local_experts
    pair_expert = expert_ids.reshape(-1)
    expert_table = (pair_expert[:, None] == jnp.arange(EXPERTS, dtype=jnp.int32)[None, :]).astype(
        jnp.int32
    )
    ranking = jnp.sum((jnp.cumsum(expert_table, axis=0) - expert_table) * expert_table, axis=1)
    local_ids = pair_expert - first_expert
    pair_token = jnp.arange(pair_expert.shape[0], dtype=jnp.int32) // 2
    matched = (
        local_ids[None, None, :] == jnp.arange(local_experts, dtype=jnp.int32)[:, None, None]
    ) & (ranking[None, None, :] == jnp.arange(SLOTS, dtype=jnp.int32)[None, :, None])
    slot_token = jnp.sum(jnp.where(matched, pair_token[None, None, :], 0), axis=2)
    filled = jnp.any(matched, axis=2)
    routed = jnp.where(filled[:, :, None], normed[slot_token], jnp.zeros((), jnp.bfloat16))
    piece = lax.all_gather(routed, "fs", axis=1, tiled=True)
    gate_part = jnp.einsum("ecd,edf->ecf", piece, gate_serving, preferred_element_type=jnp.float32)
    up_part = jnp.einsum("ecd,edf->ecf", piece, up_serving, preferred_element_type=jnp.float32)
    hidden = (jax.nn.silu(gate_part) * up_part).astype(jnp.bfloat16)
    expert_out = lax.psum_scatter(
        jnp.einsum("ecf,efd->ced", hidden, down_serving, preferred_element_type=jnp.float32).astype(
            jnp.bfloat16
        ),
        "fs",
        scatter_dimension=0,
        tiled=True,
    ).astype(jnp.float32)
    is_local = (local_ids >= 0) & (local_ids < local_experts)
    safe_local = jnp.clip(local_ids, 0, local_experts - 1)
    safe_rank = jnp.minimum(ranking, SLOTS - 1)
    picked = expert_out[safe_rank, safe_local]
    weighted = jnp.where(
        is_local[:, None], picked * route_weights.reshape(-1)[:, None], 0.0
    ).astype(jnp.bfloat16)
    weighted = weighted.reshape(token_count, 2, weighted.shape[1])
    arrived = lax.all_to_all(weighted, "tp", split_axis=0, concat_axis=1, tiled=True)
    mixed = jnp.sum(arrived.astype(jnp.float32), axis=1).astype(jnp.bfloat16)
    return (gate_serving, up_serving, down_serving, mixed)


def solution(mesh):
    in_specs = (
        P(("gr", "fs"), None),
        P(("gr", "fs"), None),
        P(("gr", "fs"), None),
        P("gr", "fs", "tp"),
        P("gr", "fs", "tp"),
        P("gr", "fs", "tp"),
        P("fs"),
    )
    out_specs = (
        P("tp", None, "fs"),
        P("tp", None, "fs"),
        P("tp", "fs", None),
        P(("gr", "fs", "tp"), None),
    )
    return jax.shard_map(body, mesh=mesh, in_specs=in_specs, out_specs=out_specs, check_vma=False)
```

profile of v0, /device:TPU:0, one launch (start us, length us, event | category | flops | bytes accessed | tf_op | source)
XLA Modules:
  0.0 1267.4 jit_solution(1871464618973655169)
XLA Ops:
  7.2 15.1 %multiply_convert_fusion = (bf16[4,256,4096]{2,1,0:T(8,128)(2,1)}, bf16[4,256,4096]{2,1,0:T(8,128)(2,1)S(1)}) fusion(f32[4,256,4096]{2,1,0:T(8,128)} %param.11, f32[256]{0:T(256)} %param.13, f32[4,256,4096]{2,1,0:T(8,128)} %param.10), kind=kLoop, calls=%fused_computation.3 | loop fusion | flops 16777216 | bytes 50332672 | tf_op jit(solution)/shard_map/convert_element_type | solution.py:26
  22.3 12.6 copy.107
  34.9 98.2 %all_to_all.135 = bf16[4,256,4096]{2,0,1:T(4,128)(2,1)} all-to-all(bf16[4,256,4096]{2,0,1:T(4,128)(2,1)S(1)} %copy.107), channel_id=1, replica_groups=mesh['gr'=2,'fs'=8,'tp'=2] {'gr'}, dimensions={1} | all-to-all | bytes 16777216 | tf_op jit(solution)/shard_map/all_to_all | solution.py:29
  133.0 11.4 copy.108
  144.4 7.9 copy.109
  152.3 6.9 all-to-all-start.1
  159.2 12.2 copy.115
  171.4 79.9 %all-to-all-done.1 = bf16[8,128,4096]{2,1,0:T(8,128)(2,1)} async-done(((bf16[8,128,4096]{2,1,0:T(8,128)(2,1)}), bf16[8,128,4096]{2,1,0:T(8,128)(2,1)}, u32[]{:S(2)}, u32[]{:S(2)}) %all-to-all-start.1) | async-done | bytes 8388640 | tf_op jit(solution)/shard_map/all_to_all | solution.py:35
  251.2 7.0 all-to-all-start.3
  258.2 11.9 copy.110
  270.2 12.1 copy.111
  282.3 67.1 %all-to-all-done.3 = bf16[4,256,4096]{2,0,1:T(4,128)(2,1)} async-done(((bf16[4,256,4096]{2,0,1:T(4,128)(2,1)}), bf16[4,256,4096]{2,0,1:T(4,128)(2,1)}, u32[]{:S(2)}, u32[]{:S(2)}) %all-to-all-start.3) | async-done | bytes 8388640 | tf_op jit(solution)/shard_map/all_to_all | solution.py:30
  349.4 5.0 all-to-all-start.2
  354.4 0.2 all-gather.9.cloned.1.call-start
  354.6 9.1 convert_element_type.42
  363.7 13.5 %copy.116 = bf16[4,256,4096]{2,1,0:T(8,128)(2,1)} copy(bf16[4,256,4096]{2,0,1:T(4,128)(2,1)} %all-to-all-done.3) | data formatting | bytes 16777216 | tf_op jit(solution)/shard_map/all_to_all | solution.py:30
  377.1 9.3 copy.117
  386.5 151.8 %all-to-all-done.2 = bf16[4,128,8192]{1,0,2:T(4,128)(2,1)} async-done(((bf16[4,128,8192]{1,0,2:T(4,128)(2,1)}), bf16[4,128,8192]{1,0,2:T(4,128)(2,1)}, u32[]{:S(2)}, u32[]{:S(2)}) %all-to-all-start.2) | async-done | bytes 8388640 | tf_op jit(solution)/shard_map/all_to_all | solution.py:34
  538.2 7.0 all-to-all-start.4
  545.3 0.0 all-gather.5.cloned.1.call-start
  545.3 7.9 copy.112
  553.2 11.3 copy.113
  564.6 73.0 %all-to-all-done.4 = bf16[8,128,4096]{2,1,0:T(8,128)(2,1)} async-done(((bf16[8,128,4096]{2,1,0:T(8,128)(2,1)}), bf16[8,128,4096]{2,1,0:T(8,128)(2,1)}, u32[]{:S(2)}, u32[]{:S(2)}) %all-to-all-start.4) | async-done | bytes 8388640 | tf_op jit(solution)/shard_map/all_to_all | solution.py:42
  637.6 11.9 copy.118
  649.5 10.1 copy.119
  659.7 187.3 %all_to_all.136 = bf16[4,128,8192]{1,0,2:T(4,128)(2,1)} all-to-all(bf16[4,128,8192]{1,0,2:T(4,128)(2,1)S(1)} %copy.119), channel_id=1, replica_groups=mesh['gr'=2,'fs'=8,'tp'=2] {'fs'}, dimensions={2} | all-to-all | bytes 16777216 | tf_op jit(solution)/shard_map/all_to_all | solution.py:41
  847.0 7.9 copy.120
  854.8 11.3 copy.121
  866.2 0.7 copy-done.1
  866.8 0.1 copy.125
  866.9 0.1 eq.65
  867.1 0.1 reshape.196
  867.2 0.6 reduce-window.6
  867.8 0.2 slice_reduce_fusion
  868.1 0.1 fusion.7
  868.2 0.2 fusion.5
  868.4 0.1 reshape.200
  868.5 0.2 fusion.3
  868.7 13.3 %all-to-all-start.6 = ((bf16[8,1024,1024]{2,1,0:T(8,128)(2,1)}), bf16[8,1024,1024]{2,1,0:T(8,128)(2,1)}, u32[]{:S(2)}, u32[]{:S(2)}) async-start(bf16[8,1024,1024]{2,1,0:T(8,128)(2,1)} %all-gather.9.cloned.1.call-done), calls=%async_computation.6 | async-start | bytes 33554432 | tf_op jit(solution)/shard_map/all_to_all | solution.py:49
  882.0 0.0 all-gather.11.cloned.1.call-start
  882.0 0.2 fusion.4
  882.2 0.9 gather_fusion
  883.1 0.2 and_reduce_fusion
  883.3 1.0 broadcast_select_fusion
  884.3 0.0 reduce-scatter.2.cloned.1.call-start
  884.3 179.9 %all-to-all-done.6 = bf16[8,1024,1024]{2,1,0:T(8,128)(2,1)} async-done(((bf16[8,1024,1024]{2,1,0:T(8,128)(2,1)}), bf16[8,1024,1024]{2,1,0:T(8,128)(2,1)}, u32[]{:S(2)}, u32[]{:S(2)}) %all-to-all-start.6) | async-done | bytes 16777248 | tf_op jit(solution)/shard_map/all_to_all | solution.py:49
  1064.2 31.0 %copy.131 = bf16[2,4,1024,1024]{3,0,2,1:T(2,128)(2,1)} copy(bf16[2,4,1024,1024]{3,2,1,0:T(8,128)(2,1)} %bitcast.24) | data formatting | bytes 33554432 | tf_op jit(solution)/shard_map/all_to_all | solution.py:49
  1095.3 27.8 %all_to_all.125 = bf16[4,1024,2048]{2,1,0:T(8,128)(2,1)} reshape(bf16[4,1024,2,1024]{3,2,1,0:T(2,128)(2,1)} %bitcast.59) | data formatting | bytes 33554432 | tf_op jit(solution)/shard_map/all_to_all | solution.py:49
  1123.1 13.9 %copy.114 = bf16[4,8,2,128,1024]{4,3,2,1,0:T(8,128)(2,1)} copy(bf16[4,8,2,128,1024]{4,3,1,2,0:T(8,128)(2,1)} %bitcast.71) | data formatting | bytes 33554432 | tf_op jit(solution)/shard_map/transpose | solution.py:18
  1137.0 13.9 %copy.122 = bf16[4,8,2,128,1024]{4,3,2,1,0:T(8,128)(2,1)} copy(bf16[4,8,2,128,1024]{4,3,1,2,0:T(8,128)(2,1)} %bitcast.72) | data formatting | bytes 33554432 | tf_op jit(solution)/shard_map/transpose | solution.py:18
  1150.9 13.5 %fusion.15 = f32[4,256,1024]{2,1,0:T(8,128)} fusion(bf16[4,256,2048]{2,1,0:T(8,128)(2,1)} %all-gather.11.cloned.1.call-done, bf16[4,2048,1024]{2,1,0:T(8,128)(2,1)} %bitcast.73), kind=kOutput, calls=%fused_computation.46 | convolution fusion | flops 4294967296 | bytes 25165824 | tf_op jit(solution)/shard_map/ecd,edf->ecf/dot_general | solution.py:77
  1164.4 19.7 %convert_bitcast_fusion = bf16[256,4,2048]{2,0,1:T(8,128)(2,1)} fusion(bf16[4,1024,2048]{2,1,0:T(8,128)(2,1)} %all_to_all.125, f32[4,256,1024]{2,1,0:T(8,128)} %fusion.15, bf16[4,256,2048]{2,1,0:T(8,128)(2,1)} %all-gather.11.cloned.1.call-done, bf16[4,2048,1024]{2,1,0:T(8,128)(2,1)} %bitcast.75), kind=kOutput, calls=%fused_computation.5 | convolution fusion | flops 8598323200 | bytes 46137344 | tf_op jit(solution)/shard_map/ecf,efd->ced/dot_general | solution.py:81
  1184.2 0.1 copy.127
  1184.3 0.1 min.31
  1184.4 0.1 copy.124
  1184.6 0.1 copy.129
  1184.7 47.2 %reduce-scatter.2.cloned.1.call-done = bf16[32,4,2048]{2,0,1:T(8,128)(2,1)} async-done(((bf16[256,4,2048]{2,0,1:T(8,128)(2,1)}), bf16[32,4,2048]{2,0,1:T(8,128)(2,1)}) %reduce-scatter.2.cloned.1.call-update) | async-done | bytes 524304 | tf_op jit(solution)/shard_map/reduce_scatter | solution.py:80
  1231.9 1.4 copy.128
  1233.4 4.2 gather_fusion.1
  1237.6 2.3 gather.10
  1239.9 2.4 select_convert_fusion
  1242.2 14.5 %all_to_all.137 = bf16[128,2,2048]{2,1,0:T(2,128)(2,1)S(1)} all-to-all(bf16[128,2,2048]{2,1,0:T(2,128)(2,1)S(1)} %select_convert_fusion), channel_id=1, replica_groups=mesh['gr'=2,'fs'=8,'tp'=2] {'tp'}, dimensions={0} | all-to-all | bytes 2097152 | tf_op jit(solution)/shard_map/all_to_all | solution.py:96
  1256.7 2.8 reduce_sum.52
  1259.5 0.8 reduce_sum.54
  (29 shorter events, 0.3 us)
Async XLA Ops:
  152.3 99.0 %all-to-all-start.1 = ((bf16[8,128,4096]{2,1,0:T(8,128)(2,1)}), bf16[8,128,4096]{2,1,0:T(8,128)(2,1)}, u32[]{:S(2)}, u32[]{:S(2)}) async-start(bf16[8,128,4096]{2,1,0:T(8,128)(2,1)} %bitcast.63), calls=%async_computation.1 | async-start | bytes 16777216 | tf_op jit(solution)/shard_map/all_to_all | solution.py:35
  251.2 98.2 %all-to-all-start.3 = ((bf16[4,256,4096]{2,0,1:T(4,128)(2,1)}), bf16[4,256,4096]{2,0,1:T(4,128)(2,1)}, u32[]{:S(2)}, u32[]{:S(2)}) async-start(bf16[4,256,4096]{2,0,1:T(4,128)(2,1)} %copy.115), calls=%async_computation.3 | async-start | bytes 16777216 | tf_op jit(solution)/shard_map/all_to_all | solution.py:30
  349.4 188.8 %all-to-all-start.2 = ((bf16[4,128,8192]{1,0,2:T(4,128)(2,1)}), bf16[4,128,8192]{1,0,2:T(4,128)(2,1)}, u32[]{:S(2)}, u32[]{:S(2)}) async-start(bf16[4,128,8192]{1,0,2:T(4,128)(2,1)} %copy.111), calls=%async_computation.2 | async-start | bytes 16777216 | tf_op jit(solution)/shard_map/all_to_all | solution.py:34
  354.4 514.3 %all-gather.9.cloned.1.call-start = ((), (), s32[]{:S(2)}) async-start(), calls=%async_computation.11 | async-start | bytes 25165824 | tf_op jit(solution)/shard_map/all_gather | solution.py:32
  538.2 99.4 %all-to-all-start.4 = ((bf16[8,128,4096]{2,1,0:T(8,128)(2,1)}), bf16[8,128,4096]{2,1,0:T(8,128)(2,1)}, u32[]{:S(2)}, u32[]{:S(2)}) async-start(bf16[8,128,4096]{2,1,0:T(8,128)(2,1)} %bitcast.62), calls=%async_computation.4 | async-start | bytes 16777216 | tf_op jit(solution)/shard_map/all_to_all | solution.py:42
  545.3 577.8 %all-gather.5.cloned.1.call-start = ((), (), s32[]{:S(2)}) async-start(), calls=%async_computation.9 | async-start | bytes 25165824 | tf_op jit(solution)/shard_map/all_gather | solution.py:51
  564.5 572.5 %all-gather.7.cloned.1.call-start = ((), (), s32[]{:S(2)}) async-start(), calls=%async_computation.10 | async-start | bytes 25165824 | tf_op jit(solution)/shard_map/all_gather | solution.py:52
  866.2 0.7 copy-start.1
  866.2 2.3 copy-start
  868.7 195.5 %all-to-all-start.6 = ((bf16[8,1024,1024]{2,1,0:T(8,128)(2,1)}), bf16[8,1024,1024]{2,1,0:T(8,128)(2,1)}, u32[]{:S(2)}, u32[]{:S(2)}) async-start(bf16[8,1024,1024]{2,1,0:T(8,128)(2,1)} %all-gather.9.cloned.1.call-done), calls=%async_computation.6 | async-start | bytes 33554432 | tf_op jit(solution)/shard_map/all_to_all | solution.py:49
  882.0 268.9 %all-gather.11.cloned.1.call-start = ((), (), s32[]{:S(2)}) async-start(), calls=%async_computation.12 | async-start | bytes 4718592 | tf_op jit(solution)/shard_map/all_gather | solution.py:76
  884.3 347.7 %reduce-scatter.2.cloned.1.call-start = ((), (), s32[]{:S(2)}) async-start(), calls=%async_computation.13 | async-start | bytes 4718592 | tf_op jit(solution)/shard_map/reduce_scatter | solution.py:80
  1164.4 20.1 %copy-start.2 = (f32[128,2]{0,1:T(2,128)S(1)}, f32[128,2]{0,1:T(2,128)}, u32[]{:S(2)}) copy-start(f32[128,2]{0,1:T(2,128)} %param.9) | copy-start | bytes 3076
Sparse Core Ops, SparseCore 0:
  363.8 198.2 all-gather.8
  564.7 198.4 all-gather.4
  866.3 195.8 all-gather.6
  1063.7 46.8 all-gather.10
  1184.3 47.5 reduce-scatter.1
where the time goes:
time: 1280 us; the launch traced here: 1270 us
  waiting for transfers between devices  599 us (47%)
  blocking collectives  300 us (23%)
  local copies, waits for them, and re-layouts  249 us (19%)
  starting transfers between devices  39.5 us (3%)
  matrix products  33.2 us (3%)
  other arithmetic  32.6 us (3%)
  between operations  14.4 us (1%)
    all_to_all x1, blocking collectives, body(): lax.all_to_all(lax.all_to_all(up_rows, 'tp', split_axis=0, concat_axis=2,...  187 us
    all_to_all x1, waiting for transfers between devices, body(): lax.all_to_all(down_whole, 'tp', split_axis=0, concat_axis=2, tiled=True)  180 us
    all_to_all x1, waiting for transfers between devices, body(): lax.all_to_all(lax.all_to_all(gate_rows, 'tp', split_axis=0, concat_axis=...  152 us
    all_to_all x1, blocking collectives, body(): lax.all_to_all(gate_local, 'gr', split_axis=1, concat_axis=0, tiled=True)  98.2 us
    all_to_all x1, waiting for transfers between devices, body(): lax.all_to_all(gate_rows, 'tp', split_axis=0, concat_axis=2, tiled=True)  79.9 us
    all_to_all x1, waiting for transfers between devices, body(): lax.all_to_all(up_rows, 'tp', split_axis=0, concat_axis=2, tiled=True)  73 us
    all_to_all x1, waiting for transfers between devices, body(): lax.all_to_all(up_local, 'gr', split_axis=1, concat_axis=0, tiled=True)  67.1 us
    all_to_all x2, local copies, waits for them, and re-layouts, body(): lax.all_to_all(down_whole, 'tp', split_axis=0, concat_axis=2, tiled=True)  58.8 us
  transfers between devices with their start and end apart: 10, of which 6 were waited for; matrix products, arithmetic and copies ran while one was open for 15% of the time, Pallas kernels for 0%

commit v1 on v0

v1 whole, which is shorter than its diff:
```python
import functools

import jax
import jax.numpy as jnp
from jax import lax
from jax.experimental import pallas as pl
from jax.experimental.pallas import tpu as pltpu
from jax.sharding import PartitionSpec as P


NORM_EPS = 1e-06
SLOTS = 32
CUT_EIGHTHS = 4


ANY = pl.BlockSpec(memory_space=pl.ANY)
SMEM = pl.BlockSpec(memory_space=pltpu.SMEM)
VMEM = pl.BlockSpec(memory_space=pltpu.VMEM)
BF16 = jnp.bfloat16
F32 = jnp.float32


def rotate(value, axis, step):
    count = lax.axis_size(axis)
    return lax.ppermute(value, axis, [(i, (i + step) % count) for i in range(count)])


def pack_kernel(parts, where_ref, after_ref, *refs):
    masters, gains, outs = refs[:parts], refs[parts : 2 * parts], refs[2 * parts :]
    for master, gain, out in zip(masters, gains, outs):
        out[0, 0] = (master[0] * gain[...]).astype(BF16)


def pack(master, gain, where, unit, units, width, parts, after):
    _, rows, cols = master.shape
    held, blocks, part_rows = master.shape[0] // units, cols // width, rows // parts

    def row_part(p):
        return lambda k, c, w: (k * units + unit, (w[0] + p) % parts, c)

    def gain_part(p):
        return lambda k, c, w: ((w[0] + p) % parts, 0)

    out_spec = pl.BlockSpec((1, 1, part_rows, width), lambda k, c, w: (k, c, 0, 0))
    return pl.pallas_call(
        functools.partial(pack_kernel, parts),
        grid_spec=pltpu.PrefetchScalarGridSpec(
            num_scalar_prefetch=1,
            grid=(held, blocks),
            in_specs=[ANY]
            + [pl.BlockSpec((1, part_rows, width), row_part(p)) for p in range(parts)]
            + [pl.BlockSpec((part_rows, 1), gain_part(p)) for p in range(parts)],
            out_specs=[out_spec] * parts,
        ),
        out_shape=[jax.ShapeDtypeStruct((held, blocks, part_rows, width), BF16)] * parts,
        name="pack",
    )(where, after, *([master] * parts), *([gain] * parts))


def choose_kernel(group_count, tp_count, held, tp_step, where_ref, after_ref, *refs):
    by_gr, (out, stage, sem) = refs[:group_count], refs[group_count:]
    target = lax.rem(where_ref[2] + tp_step, tp_count)
    gr_step = lax.rem(where_ref[0] + group_count - lax.div(target, held), group_count)
    for s in range(group_count):

        @pl.when(gr_step == s)
        def _(s=s):
            copy = pltpu.make_async_copy(by_gr[s].at[lax.rem(target, held)], stage, sem)
            copy.start()
            copy.wait()

    copy = pltpu.make_async_copy(stage, out, sem)
    copy.start()
    copy.wait()


def choose(by_gr, where, tp_step, after):
    held, *shape = by_gr[0].shape
    return pl.pallas_call(
        functools.partial(choose_kernel, len(by_gr), lax.axis_size("tp"), held, tp_step),
        in_specs=[SMEM] + [ANY] * (len(by_gr) + 1),
        out_specs=ANY,
        out_shape=jax.ShapeDtypeStruct(tuple(shape), BF16),
        scratch_shapes=[pltpu.VMEM(tuple(shape), BF16), pltpu.SemaphoreType.DMA],
        name="choose",
    )(where, after, *by_gr)


def stack_kernel(count, after_ref, *refs):
    ins, (out, stage, in_sem, out_sem) = refs[:count], refs[count:]

    def fetch(i):
        return pltpu.make_async_copy(ins[i], stage.at[i], in_sem.at[i])

    def flush(i):
        return pltpu.make_async_copy(stage.at[i], out.at[i], out_sem.at[i])

    for i in range(count):
        fetch(i).start()
    for i in range(count):
        fetch(i).wait()
        flush(i).start()
    for i in range(count):
        flush(i).wait()


def stack(values, after):
    count, shape = len(values), (len(values), *values[0].shape)
    return pl.pallas_call(
        functools.partial(stack_kernel, count),
        in_specs=[ANY] * (count + 1),
        out_specs=ANY,
        out_shape=jax.ShapeDtypeStruct(shape, BF16),
        scratch_shapes=[
            pltpu.VMEM(shape, BF16),
            pltpu.SemaphoreType.DMA((count,)),
            pltpu.SemaphoreType.DMA((count,)),
        ],
        name="stack",
    )(after, *values)


def split_kernel(group_count, tp_count, shard_count, held, where_ref, after_ref, *refs):
    by_gr, by_tp = refs[:group_count], refs[group_count : group_count + tp_count - 1]
    outs = refs[group_count + tp_count - 1 : group_count + tp_count - 1 + shard_count]
    stage, in_sem, out_sem = refs[-3:]
    g, f, t = where_ref[0], where_ref[1], where_ref[2]
    blocks = by_gr[0].shape[1]

    def source(step):
        target = lax.rem(f + step, shard_count)
        return lax.div(target, blocks), lax.rem(target, blocks)

    for step in range(shard_count):
        column, block = source(step)
        own_gr = lax.rem(g + group_count - lax.div(t, held), group_count)
        tp_step = lax.rem(t + tp_count - column, tp_count)
        for s in range(group_count):

            @pl.when((tp_step == 0) & (own_gr == s))
            def _(s=s):
                pltpu.make_async_copy(
                    by_gr[s].at[lax.rem(t, held), block], stage.at[step], in_sem.at[step]
                ).start()

        for s in range(1, tp_count):

            @pl.when(tp_step == s)
            def _(s=s):
                pltpu.make_async_copy(by_tp[s - 1].at[block], stage.at[step], in_sem.at[step]).start()

    for step in range(shard_count):
        pltpu.make_async_copy(stage.at[step], stage.at[step], in_sem.at[step]).wait()
        pltpu.make_async_copy(stage.at[step], outs[step], out_sem.at[step]).start()
    for step in range(shard_count):
        pltpu.make_async_copy(stage.at[step], outs[step], out_sem.at[step]).wait()


def split(by_gr, by_tp, where, shard_count, after):
    held, _, rows, width = by_gr[0].shape
    piece = jax.ShapeDtypeStruct((rows, width), BF16)
    return pl.pallas_call(
        functools.partial(split_kernel, len(by_gr), len(by_tp) + 1, shard_count, held),
        in_specs=[SMEM] + [ANY] * (len(by_gr) + len(by_tp) + 1),
        out_specs=[ANY] * shard_count,
        out_shape=[piece] * shard_count,
        scratch_shapes=[
            pltpu.VMEM((shard_count, rows, width), BF16),
            pltpu.SemaphoreType.DMA((shard_count,)),
            pltpu.SemaphoreType.DMA((shard_count,)),
        ],
        name="split",
    )(where, after, *by_gr, *by_tp)


def up_kernel(counts, shard_count, parts, unit, fresh, where_ref, after_ref, near, far, *refs):
    gate_in, up_in = refs[: counts[0]], refs[counts[0] : sum(counts)]
    rest = refs[sum(counts) :]
    if not fresh:
        rest = rest[2:]
    gate_out, up_out, hidden_ref, tokens, gate_buf, up_buf, token_sem, in_sem, out_sem = rest
    g, f = where_ref[0], where_ref[1]
    whole = gate_buf.shape[0] // shard_count
    sides = ((gate_in, gate_buf, gate_out), (up_in, up_buf, up_out))

    def place(index, side):
        part, step = divmod(index, shard_count)
        rows = whole // parts[side]
        source = lax.rem(f + shard_count - step, shard_count)
        start = source * whole + lax.rem(g + parts[side] - part, parts[side]) * rows
        return pl.ds(pl.multiple_of(start, rows), rows)

    def fetch(index, side):
        ins, buf, _ = sides[side]
        part, step = divmod(index, shard_count)
        src = ins[index] if parts[side] == 1 else ins[part].at[step]
        return pltpu.make_async_copy(src, buf.at[place(index, side)], in_sem.at[side, index])

    def flush(index, side):
        _, buf, out = sides[side]
        at = place(index, side)
        return pltpu.make_async_copy(buf.at[at], out.at[unit, at, :], out_sem.at[side, index])

    outer, slots, depth = near.shape[0], tokens.shape[1], tokens.shape[2]
    rows_of_unit = pl.ds(unit * slots, slots)
    token_copies = [
        pltpu.make_async_copy(
            src.at[:, rows_of_unit, :], tokens.at[pl.ds(i * outer, outer)], token_sem.at[i]
        )
        for i, src in enumerate((near, far))
    ]
    for copy in token_copies:
        copy.start()
    for side in (0, 1):
        for index in range(shard_count * parts[side]):
            fetch(index, side).start()
    for copy in token_copies:
        copy.wait()
    rows_in = tokens[...].reshape(2 * outer * slots, depth)
    products = []
    for side in (0, 1):
        for index in range(shard_count * parts[side]):
            fetch(index, side).wait()
            flush(index, side).start()
        products.append(jnp.dot(rows_in, sides[side][1][...], preferred_element_type=F32))
    gate, up = products
    hidden_ref[...] = (gate / (1.0 + jnp.exp(-gate)) * up).astype(BF16)
    for side in (0, 1):
        for index in range(shard_count * parts[side]):
            flush(index, side).wait()


def up_project(where, near, far, gate_pieces, up_pieces, outs, unit, parts, out_shape, after):
    width = out_shape.shape[2]
    shard_count, depth = 2 * near.shape[0], near.shape[2]
    slots = near.shape[1] // out_shape.shape[0]
    token_count = shard_count * slots
    counts = (len(gate_pieces), len(up_pieces))
    fresh = outs is None
    operands = [where, after, near, far, *gate_pieces, *up_pieces] + ([] if fresh else list(outs))
    return pl.pallas_call(
        functools.partial(up_kernel, counts, shard_count, parts, unit, fresh),
        in_specs=[SMEM] + [ANY] * (len(operands) - 1),
        out_specs=[ANY, ANY, VMEM],
        out_shape=[out_shape, out_shape, jax.ShapeDtypeStruct((token_count, width), BF16)],
        scratch_shapes=[
            pltpu.VMEM((shard_count, slots, depth), BF16),
            pltpu.VMEM((depth, width), BF16),
            pltpu.VMEM((depth, width), BF16),
            pltpu.SemaphoreType.DMA((2,)),
            pltpu.SemaphoreType.DMA((2, shard_count * max(parts))),
            pltpu.SemaphoreType.DMA((2, shard_count * max(parts))),
        ],
        input_output_aliases={} if fresh else {4 + sum(counts): 0, 5 + sum(counts): 1},
        name="up_project",
    )(*operands)


def down_kernel(group_count, tp_count, held, unit, fresh, where_ref, after_ref, hidden_ref, *refs):
    by_gr, by_tp = refs[:group_count], refs[group_count : group_count + tp_count - 1]
    rest = refs[group_count + tp_count - 1 :]
    if not fresh:
        rest = rest[1:]
    down_out, near_ref, far_ref, buf, part, in_sem, out_sem = rest
    g, t = where_ref[0], where_ref[2]
    cols = buf.shape[2]
    own_gr = lax.rem(g + group_count - lax.div(t, held), group_count)
    for s in range(group_count):

        @pl.when(own_gr == s)
        def _(s=s):
            pltpu.make_async_copy(by_gr[s].at[lax.rem(t, held)], buf.at[0], in_sem.at[0]).start()

    for s in range(1, tp_count):
        pltpu.make_async_copy(by_tp[s - 1], buf.at[s], in_sem.at[s]).start()

    def flush(s):
        column = pl.multiple_of(lax.rem(t + tp_count - s, tp_count) * cols, cols)
        return pltpu.make_async_copy(
            buf.at[s], down_out.at[unit, :, pl.ds(column, cols)], out_sem.at[s]
        )

    for s in range(tp_count):
        pltpu.make_async_copy(buf.at[s], buf.at[s], in_sem.at[s]).wait()
        flush(s).start()
        column = pl.multiple_of(lax.rem(t + tp_count - s, tp_count) * cols, cols)
        part[:, pl.ds(column, cols)] = jnp.dot(
            hidden_ref[...], buf[s], preferred_element_type=F32
        ).astype(BF16)
    half = near_ref.shape[0]
    near_ref[...] = part[:half]
    far_ref[...] = part[half:]
    for s in range(tp_count):
        flush(s).wait()


def down_project(where, hidden, by_gr, by_tp, out, unit, out_shape, after):
    held, rows, cols = by_gr[0].shape
    token_count, _ = hidden.shape
    tp_count = len(by_tp) + 1
    depth = cols * tp_count
    fresh = out is None
    half = jax.ShapeDtypeStruct((token_count // 2, depth), BF16)
    operands = [where, after, hidden, *by_gr, *by_tp] + ([] if fresh else [out])
    return pl.pallas_call(
        functools.partial(down_kernel, len(by_gr), tp_count, held, unit, fresh),
        in_specs=[SMEM, ANY, VMEM] + [ANY] * (len(operands) - 3),
        out_specs=[ANY, VMEM, VMEM],
        out_shape=[out_shape, half, half],
        scratch_shapes=[
            pltpu.VMEM((tp_count, rows, cols), BF16),
            pltpu.VMEM((token_count, depth), BF16),
            pltpu.SemaphoreType.DMA((tp_count,)),
            pltpu.SemaphoreType.DMA((tp_count,)),
        ],
        input_output_aliases={} if fresh else {len(operands) - 1: 0},
        name="down_project",
    )(*operands)


def fold_kernel(outer, after_ref, keep_ref, other_ref, own_ref, *sends):
    total = keep_ref[...].astype(F32) + other_ref[...].astype(F32)
    slots = own_ref.shape[0]
    own_ref[...] = total[:slots]
    for step in range(1, outer):
        sends[step - 1][...] = total[step * slots : (step + 1) * slots].astype(BF16)


def fold(keep, other, outer, after):
    slots, depth = keep.shape[0] // outer, keep.shape[1]
    return pl.pallas_call(
        functools.partial(fold_kernel, outer),
        in_specs=[ANY, VMEM, VMEM],
        out_specs=[VMEM] * outer,
        out_shape=[jax.ShapeDtypeStruct((slots, depth), F32)]
        + [jax.ShapeDtypeStruct((slots, depth), BF16)] * (outer - 1),
        name="fold",
    )(after, keep, other)


def combine_kernel(count, first, after_ref, weight_ref, onehot_ref, own_ref, *refs):
    others, (mixed_ref, out_ref) = refs[:count], refs[-2:]
    total = own_ref[...]
    for other in others:
        total = total + other[...].astype(F32)
    term = (total * weight_ref[...]).astype(BF16)
    share = lax.dot_general(
        onehot_ref[...], term, (((1,), (0,)), ((), ())), preferred_element_type=F32
    )
    out_ref[...] = share if first else mixed_ref[...] + share


def combine(weight, onehot, own, others, mixed, after):
    shape = jax.ShapeDtypeStruct((onehot.shape[0], own.shape[1]), F32)
    first = mixed is None
    operands = [after, weight, onehot, own, *others, own if first else mixed]
    return pl.pallas_call(
        functools.partial(combine_kernel, len(others), first),
        in_specs=[ANY] + [VMEM] * (len(operands) - 1),
        out_specs=VMEM,
        out_shape=shape,
        name="combine",
    )(*operands)


def cast_kernel(after_ref, in_ref, out_ref):
    out_ref[...] = in_ref[...].astype(BF16)


def cast(master, unit, units, after):
    local_in, rows, cols = master.shape
    held, half = local_in // units, rows // 2
    return pl.pallas_call(
        cast_kernel,
        grid=(held, 2),
        in_specs=[ANY, pl.BlockSpec((1, half, cols), lambda k, i: (k * units + unit, i, 0))],
        out_specs=pl.BlockSpec((1, half, cols), lambda k, i: (k, i, 0)),
        out_shape=jax.ShapeDtypeStruct((held, rows, cols), BF16),
        name="cast",
    )(after, master)


def plan(units, cut):
    both = (0, 1)
    keys = [(which, unit) for unit in range(units) for which in both]
    first = [key for key in keys if key in cut]
    second = [key for key in keys if key not in cut]
    cut_rank = {unit: sum((which, unit) in cut for which in both) for unit in range(units)}
    downs = sorted(range(units), key=lambda unit: (cut_rank[unit], unit))
    events = []
    y = x = z = 0.3
    ready = {}
    for i, key in enumerate(first):
        events.append((0.2 * i, "pack", key))
        y = max(y, 0.2 * i + 0.3) + 1
        ready["y", key] = y
    start = 0.2 * min(2, len(first))
    events.append((start + 0.01, "tokens", None))
    z = start + 2.3
    events.append((z, "near", None))
    for i, key in enumerate(second):
        at = max(0.2 * len(first), 0.9) + 0.3 * i
        events.append((at, "pack", key))
        y = max(y, at + 0.3) + 2
        ready["y", key] = y
    for i, unit in enumerate(downs):
        events.append((max(0.2 * len(first), 0.9) + 0.3 * (len(second) + i) + 0.2, "cast", unit))
        y = y + 2
        ready["y", unit] = y
    for key in first + second + downs:
        size = 1 if key in first else 2
        at = ready["y", key]
        events.append((at, "choose", key))
        x = max(x, at + 0.2) + size
        ready["x", key] = x
        if key not in downs:
            events.append((x, "split", key))
            z = max(z, x + 0.2) + 2 * size
            ready["z", key] = z
    for key in first:
        at = ready["z", key]
        events.append((at, "stack", key))
        y = max(y, at + 0.2) + 2
        ready["z", key] = y
    order = sorted(range(units), key=lambda unit: max(ready["z", (which, unit)] for which in both))
    now = 0.0
    for unit in order:
        at = max(now, ready["x", unit], *(ready["z", (which, unit)] for which in both))
        now = at + 0.7
        events.append((at, "project", unit))
        z = max(z, at + 0.7) + 0.5
        events.append((z + 0.3, "settle", unit))
    events.sort(key=lambda event: event[0])
    return [event[1:] for event in events]


def body(prompt, expert_ids, route_weights, gate_master, up_master, down_master, ffn_gain):
    group_count, shard_count, tp_count = (lax.axis_size(name) for name in ("gr", "fs", "tp"))
    g, f, t = (lax.axis_index(name) for name in ("gr", "fs", "tp"))
    where = jnp.stack([g, f, t]).astype(jnp.int32)
    local_in, rows, cols = gate_master.shape
    units = local_in * group_count // tp_count
    width = cols * tp_count // shard_count
    depth = prompt.shape[1]
    gain = ffn_gain.reshape(rows, 1)
    cut = [(which, unit) for unit in range(units) for which in (0, 1)][: units * CUT_EIGHTHS // 4]
    parts_of = {
        (which, unit): group_count if (which, unit) in cut else 1
        for unit in range(units)
        for which in (0, 1)
    }
    masters = (gate_master, up_master)
    serving = jax.ShapeDtypeStruct((units, rows * shard_count, width), BF16)
    down_serving = jax.ShapeDtypeStruct((units, *down_master.shape[1:2], depth), BF16)
    outer = shard_count // 2
    pairs = [(i, i ^ 1) for i in range(shard_count)]

    token_count = prompt.shape[0]
    xfloat = prompt.astype(F32)
    normed = (
        xfloat * lax.rsqrt(jnp.mean(xfloat * xfloat, axis=1, keepdims=True) + NORM_EPS)
    ).astype(BF16)
    local_experts = t * units + jnp.arange(units, dtype=jnp.int32)
    named = expert_ids[:, :, None] == local_experts[None, None, :]
    chosen = jnp.any(named, axis=1)
    earlier = jnp.tril(jnp.ones((token_count, token_count), BF16), -1)
    rank = jnp.dot(earlier, chosen.astype(BF16), preferred_element_type=F32).astype(jnp.int32)
    slot_ids = jnp.arange(SLOTS, dtype=jnp.int32)
    table = chosen.T[:, None, :] & (rank.T[:, None, :] == slot_ids[None, :, None])
    pair_weight = jnp.sum(jnp.where(named, route_weights[:, :, None], 0.0), axis=1)
    slot_weight = jnp.sum(jnp.where(table, pair_weight.T[:, None, :], 0.0), axis=2)[:, :, None]
    onehot = table.astype(BF16)
    token_onehot = onehot.transpose(0, 2, 1)
    routed = jnp.dot(
        onehot.reshape(units * SLOTS, token_count), normed, preferred_element_type=F32
    ).astype(BF16)

    last, count = routed, 0

    def step(kernel, *args):
        nonlocal last, count
        count += 1
        out = kernel(*args, last)
        last = out[-1] if isinstance(out, (list, tuple)) else out
        return out

    def swap(value):
        return lax.ppermute(value, "fs", pairs)

    by_gr, by_tp, arrived, pieces, folded = {}, {}, {}, {}, {}
    projections, down, mixed = None, None, None
    last = expert_ids
    for kind, key in plan(units, cut):
        if kind == "pack":
            which, unit = key
            parts = parts_of[key]
            packed = step(pack, masters[which], gain, where, unit, units, width, parts)
            by_gr[key] = [packed[0]] + [
                rotate(packed[shift % parts], "gr", shift) for shift in range(1, group_count)
            ]
        elif kind == "cast":
            own = step(cast, down_master, key, units)
            by_gr[key] = [own] + [rotate(own, "gr", shift) for shift in range(1, group_count)]
        elif kind == "tokens":
            last, routed = lax.optimization_barrier((last, routed))
            near_parts = [routed] + [rotate(routed, "fs", 2 * shift) for shift in range(1, outer)]
            last = routed
        elif kind == "near":
            near = step(stack, near_parts)
            far = swap(near)
        elif kind == "choose":
            by_tp[key] = []
            for shift in range(1, tp_count):
                by_tp[key].append(rotate(step(choose, by_gr[key], where, shift), "tp", shift))
        elif kind == "split":
            blocks = step(split, by_gr[key], by_tp[key], where, shard_count)
            arrived[key] = [blocks[0]] + [
                rotate(blocks[shift], "fs", shift) for shift in range(1, shard_count)
            ]
            if key not in cut:
                pieces[key] = arrived[key]
        elif kind == "stack":
            own = step(stack, arrived[key])
            pieces[key] = [own] + [rotate(own, "gr", shift) for shift in range(1, group_count)]
        elif kind == "project":
            parts = (parts_of[0, key], parts_of[1, key])
            *projections, hidden = step(
                up_project, where, near, far, pieces[0, key], pieces[1, key], projections, key, parts, serving
            )
            down, keep, out = step(
                down_project, where, hidden, by_gr[key], by_tp[key], down, key, down_serving
            )
            other = swap(out)
            sums = step(fold, keep, other, outer)
            folded[key] = (
                sums[0],
                [rotate(sums[shift], "fs", -2 * shift) for shift in range(1, outer)],
            )
        else:
            mixed = step(combine, slot_weight[key], token_onehot[key], *folded[key], mixed)

    mixed = mixed.reshape(tp_count, token_count // tp_count, depth)
    result = lax.dynamic_index_in_dim(mixed, t, 0, keepdims=False)
    for step in range(1, tp_count):
        target = lax.rem(t + step, tp_count)
        result = result + rotate(
            lax.dynamic_index_in_dim(mixed, target, 0, keepdims=False), "tp", step
        )
    return (*projections, down, result.astype(BF16))


def solution(mesh):
    in_specs = (
        P(("gr", "fs"), None),
        P(("gr", "fs"), None),
        P(("gr", "fs"), None),
        P("gr", "fs", "tp"),
        P("gr", "fs", "tp"),
        P("gr", "fs", "tp"),
        P("fs"),
    )
    out_specs = (
        P("tp", None, "fs"),
        P("tp", None, "fs"),
        P("tp", "fs", None),
        P(("gr", "fs", "tp"), None),
    )

    return jax.shard_map(body, mesh=mesh, in_specs=in_specs, out_specs=out_specs, check_vma=False)
```

time: 1280 us -> 1100 us (0.86)
  starting transfers between devices: 39.5 us -> 343 us
  blocking collectives: 300 us -> 0 us
  local copies, waits for them, and re-layouts: 249 us -> 14.1 us
  Pallas kernels: 0 us -> 214 us
  waiting for transfers between devices: 599 us -> 516 us
  matrix products: 33.2 us -> 1.4 us
  other arithmetic: 32.6 us -> 3.14 us
    all_to_all x5 -> x0, waiting for transfers between devices: 552 us -> none  [the longest x1 180 us: body(): lax.all_to_all(down_whole, 'tp', split_axis=0, concat_axis=2, tiled=True)]
    ppermute x0 -> x105, waiting for transfers between devices: none -> 516 us  [the longest x100 515 us: rotate(): lax.ppermute(value, axis, [(i, (i + step) % count) for i in range(count)])]
    ppermute x0 -> x105, starting transfers between devices: none -> 343 us  [the longest x100 340 us: rotate(): lax.ppermute(value, axis, [(i, (i + step) % count) for i in range(count)])]
    all_to_all x3 -> x0, blocking collectives: 300 us -> none  [the longest x1 187 us: body(): lax.all_to_all(lax.all_to_all(up_rows, 'tp', split_axis=0, concat_axis=2,...]
    pallas_call x0 -> x53, Pallas kernels: none -> 214 us  [the longest x12 40.9 us: choose(): pl.pallas_call(functools.partial(choose_kernel, len(by_gr), lax.axis_size...]
    all_to_all x14 -> x0, local copies, waits for them, and re-layouts: 185 us -> none  [the longest x2 58.8 us: body(): lax.all_to_all(down_whole, 'tp', split_axis=0, concat_axis=2, tiled=True)]
    reduce_scatter x1 -> x0, waiting for transfers between devices: 47.2 us -> none  [body(): lax.psum_scatter(jnp.einsum('ecf,efd->ced', hidden, down_serving, preferr...]
    all_to_all x5 -> x0, starting transfers between devices: 39.2 us -> none  [the longest x1 13.3 us: body(): lax.all_to_all(down_whole, 'tp', split_axis=0, concat_axis=2, tiled=True)]
  transfers between devices with their start and end apart: 10 -> 105, of which waited for: 6 -> 42; matrix products, arithmetic and copies ran while one was open for 15% -> 1% of each run, Pallas kernels for 0% -> 18%
where the time goes in v1:
time: 1100 us; the launch traced here: 1090 us
  waiting for transfers between devices  516 us (47%)
  starting transfers between devices  343 us (31%)
  Pallas kernels  214 us (19%)
  local copies, waits for them, and re-layouts  14.1 us (1%)
    ppermute x100, waiting for transfers between devices, rotate(): lax.ppermute(value, axis, [(i, (i + step) % count) for i in range(count)])  515 us
    ppermute x100, starting transfers between devices, rotate(): lax.ppermute(value, axis, [(i, (i + step) % count) for i in range(count)])  340 us
    pallas_call x12, Pallas kernels, choose(): pl.pallas_call(functools.partial(choose_kernel, len(by_gr), lax.axis_size...  40.9 us
    pallas_call x8, Pallas kernels, pack(): pl.pallas_call(functools.partial(pack_kernel, parts), grid_spec=pltpu.Pre...  40.3 us
    pallas_call x4, Pallas kernels, up_project(): pl.pallas_call(functools.partial(up_kernel, counts, shard_count, parts, u...  35.2 us
    pallas_call x8, Pallas kernels, split(): pl.pallas_call(functools.partial(split_kernel, len(by_gr), len(by_tp) + 1...  29.8 us
    pallas_call x4, Pallas kernels, down_project(): pl.pallas_call(functools.partial(down_kernel, len(by_gr), tp_count, held,...  23.1 us
  transfers between devices with their start and end apart: 105, of which 42 were waited for; matrix products, arithmetic and copies ran while one was open for 1% of the time, Pallas kernels for 18%

profile of v1, /device:TPU:0, one launch (start us, length us, event | category | flops | bytes accessed | tf_op | source)
XLA Modules:
  0.0 1093.5 jit_solution(9271408702066774755)
XLA Ops:
  4.1 5.1 pack.8
  12.5 5.0 pack.9
  17.5 5.1 pack.10
  28.9 4.9 pack.11
  33.8 5.0 pack.12.after_ref.refs_0_
  38.8 5.0 pack.13.after_ref.refs_0_
  51.5 10.7 collective-permute-done.4.refs_2_
  63.8 12.5 %collective-permute-done.5.refs_3_ = bf16[128,2048]{1,0:T(8,128)(2,1)} collective-permute-done((bf16[128,2048]{1,0:T(8,128)(2,1)}, bf16[128,2048]{1,0:T(8,128)(2,1)}, u32[]{:S(2)}, u32[]{:S(2)}) %collective-permute-start.5) | collective-permute-done | bytes 524320 | tf_op jit(solution)/shard_map/ppermute | solution.py:25
  76.9 5.0 pack.14.after_ref.refs_0_
  81.9 5.0 pack.15.after_ref.refs_0_
  99.5 71.8 %collective-permute-done.6.refs_1_ = bf16[1,4,128,1024]{3,2,1,0:T(8,128)(2,1)S(1)} collective-permute-done((bf16[1,4,128,1024]{3,2,1,0:T(8,128)(2,1)}, bf16[1,4,128,1024]{3,2,1,0:T(8,128)(2,1)S(1)}, u32[]{:S(2)}, u32[]{:S(2)}) %collective-permute-start.6) | collective-permute-done | bytes 1048608 | tf_op jit(solution)/shard_map/ppermute | solution.py:25
  171.2 21.7 %collective-permute-done.8.refs_1_ = bf16[1,4,128,1024]{3,2,1,0:T(8,128)(2,1)} collective-permute-done((bf16[1,4,128,1024]{3,2,1,0:T(8,128)(2,1)}, bf16[1,4,128,1024]{3,2,1,0:T(8,128)(2,1)}, u32[]{:S(2)}, u32[]{:S(2)}) %collective-permute-start.8) | collective-permute-done | bytes 1048608 | tf_op jit(solution)/shard_map/ppermute | solution.py:25
  225.8 16.9 %collective-permute-start.20 = (bf16[128,1024]{1,0:T(8,128)(2,1)}, bf16[128,1024]{1,0:T(8,128)(2,1)S(1)}, u32[]{:S(2)}, u32[]{:S(2)}) collective-permute-start(bf16[128,1024]{1,0:T(8,128)(2,1)} %get-tuple-element.139), channel_id=1, source_target_pairs={{0,4},{2,6},{4,8},{6,10},{8,12},{10,14},{12,0},{14,2},{1,5},{3,7},... | collective-permute-start | bytes 786440 | tf_op jit(solution)/shard_map/ppermute | solution.py:25
  244.1 6.1 collective-permute-done.20.refs_2_
  251.2 16.4 %collective-permute-done.21.refs_3_ = bf16[128,1024]{1,0:T(8,128)(2,1)S(1)} collective-permute-done((bf16[128,1024]{1,0:T(8,128)(2,1)}, bf16[128,1024]{1,0:T(8,128)(2,1)S(1)}, u32[]{:S(2)}, u32[]{:S(2)}) %collective-permute-start.21) | collective-permute-done | bytes 262176 | tf_op jit(solution)/shard_map/ppermute | solution.py:25
  269.3 8.9 collective-permute-done.23.refs_5_
  286.7 16.1 %collective-permute-start.25 = (bf16[128,1024]{1,0:T(8,128)(2,1)}, bf16[128,1024]{1,0:T(8,128)(2,1)S(1)}, u32[]{:S(2)}, u32[]{:S(2)}) collective-permute-start(bf16[128,1024]{1,0:T(8,128)(2,1)} %get-tuple-element.126.after_ref), channel_id=1, source_target_pairs={{0,14},{2,0},{4,2},{6,4},{8,6},{10,8},{12,10},{14,12},{1,15},{3,1}... | collective-permute-start | bytes 786440 | tf_op jit(solution)/shard_map/ppermute | solution.py:25
  312.8 10.1 collective-permute-start.48
  332.4 20.3 %collective-permute-done.46.refs_1_ = bf16[1,1024,1024]{2,1,0:T(8,128)(2,1)} collective-permute-done((bf16[1,1024,1024]{2,1,0:T(8,128)(2,1)S(1)}, bf16[1,1024,1024]{2,1,0:T(8,128)(2,1)}, u32[]{:S(2)}, u32[]{:S(2)}) %collective-permute-start.46) | collective-permute-done | bytes 2097184 | tf_op jit(solution)/shard_map/ppermute | solution.py:25
  354.2 12.9 %collective-permute-start.30 = (bf16[128,1024]{1,0:T(8,128)(2,1)S(1)}, bf16[128,1024]{1,0:T(8,128)(2,1)S(1)}, u32[]{:S(2)}, u32[]{:S(2)}) collective-permute-start(bf16[128,1024]{1,0:T(8,128)(2,1)S(1)} %copy-done.60), channel_id=1, source_target_pairs={{0,6},{2,8},{4,10},{6,12},{8,14},{10,0},{12,2},{14,4},{1,7},{3,9},... | collective-permute-start | bytes 786440 | tf_op jit(solution)/shard_map/ppermute | solution.py:25
  367.1 6.4 collective-permute-start.31
  375.0 16.1 %collective-permute-start.32 = (bf16[128,1024]{1,0:T(8,128)(2,1)}, bf16[128,1024]{1,0:T(8,128)(2,1)S(1)}, u32[]{:S(2)}, u32[]{:S(2)}) collective-permute-start(bf16[128,1024]{1,0:T(8,128)(2,1)} %get-tuple-element.150), channel_id=1, source_target_pairs={{0,10},{2,12},{4,14},{6,0},{8,2},{10,4},{12,6},{14,8},{1,11},{3,13... | collective-permute-start | bytes 786440 | tf_op jit(solution)/shard_map/ppermute | solution.py:25
  391.1 12.3 %collective-permute-start.33 = (bf16[128,1024]{1,0:T(8,128)(2,1)}, bf16[128,1024]{1,0:T(8,128)(2,1)S(1)}, u32[]{:S(2)}, u32[]{:S(2)}) collective-permute-start(bf16[128,1024]{1,0:T(8,128)(2,1)} %get-tuple-element.151), channel_id=1, source_target_pairs={{0,12},{2,14},{4,0},{6,2},{8,4},{10,6},{12,8},{14,10},{1,13},{3,15... | collective-permute-start | bytes 786440 | tf_op jit(solution)/shard_map/ppermute | solution.py:25
  409.6 4.9 collective-permute-done.34.refs_7_
  418.8 7.0 collective-permute-done.38.refs_2_
  425.9 16.1 %collective-permute-done.39.refs_3_ = bf16[128,1024]{1,0:T(8,128)(2,1)} collective-permute-done((bf16[128,1024]{1,0:T(8,128)(2,1)}, bf16[128,1024]{1,0:T(8,128)(2,1)}, u32[]{:S(2)}, u32[]{:S(2)}) %collective-permute-start.39) | collective-permute-done | bytes 262176 | tf_op jit(solution)/shard_map/ppermute | solution.py:25
  448.9 4.3 collective-permute-done.41.refs_5_
  453.2 6.6 collective-permute-done.42.refs_6_
  471.0 4.3 split.12
  481.4 14.7 %collective-permute-done.36.refs_2_ = bf16[4,256,1024]{2,1,0:T(8,128)(2,1)} collective-permute-done((bf16[4,256,1024]{2,1,0:T(8,128)(2,1)}, bf16[4,256,1024]{2,1,0:T(8,128)(2,1)}, u32[]{:S(2)}, u32[]{:S(2)}) %collective-permute-start.36) | collective-permute-done | bytes 2097184 | tf_op jit(solution)/shard_map/ppermute | solution.py:25
  496.6 4.3 split.13
  508.0 8.2 collective-permute-done.67.refs_1_
  516.8 44.4 %collective-permute-done.69.refs_3_ = bf16[8,128,1024]{2,1,0:T(8,128)(2,1)} collective-permute-done((bf16[8,128,1024]{2,1,0:T(8,128)(2,1)}, bf16[8,128,1024]{2,1,0:T(8,128)(2,1)}, u32[]{:S(2)}, u32[]{:S(2)}) %collective-permute-start.69) | collective-permute-done | bytes 2097184 | tf_op jit(solution)/shard_map/ppermute | solution.py:25
  561.2 44.4 %collective-permute-done.68.refs_1_ = bf16[8,128,1024]{2,1,0:T(8,128)(2,1)} collective-permute-done((bf16[8,128,1024]{2,1,0:T(8,128)(2,1)}, bf16[8,128,1024]{2,1,0:T(8,128)(2,1)}, u32[]{:S(2)}, u32[]{:S(2)}) %collective-permute-start.68) | collective-permute-done | bytes 2097184 | tf_op jit(solution)/shard_map/ppermute | solution.py:25
  609.5 39.1 %collective-permute-done.60.refs_11_ = bf16[256,1024]{1,0:T(8,128)(2,1)} collective-permute-done((bf16[256,1024]{1,0:T(8,128)(2,1)S(1)}, bf16[256,1024]{1,0:T(8,128)(2,1)}, u32[]{:S(2)}, u32[]{:S(2)}) %collective-permute-start.60) | collective-permute-done | bytes 524320 | tf_op jit(solution)/shard_map/ppermute | solution.py:25
  648.7 8.9 collective-permute-start.63
  657.5 16.4 %collective-permute-start.64 = (bf16[256,1024]{1,0:T(8,128)(2,1)S(1)}, bf16[256,1024]{1,0:T(8,128)(2,1)}, u32[]{:S(2)}, u32[]{:S(2)}) collective-permute-start(bf16[256,1024]{1,0:T(8,128)(2,1)S(1)} %copy-done.17), channel_id=1, source_target_pairs={{0,14},{2,0},{4,2},{6,4},{8,6},{10,8},{12,10},{14,12},{1,15},{3,1}... | collective-permute-start | bytes 1572872 | tf_op jit(solution)/shard_map/ppermute | solution.py:25
  679.6 4.3 split.14
  690.5 28.0 %collective-permute-start.54 = (bf16[256,1024]{1,0:T(8,128)(2,1)}, bf16[256,1024]{1,0:T(8,128)(2,1)}, u32[]{:S(2)}, u32[]{:S(2)}) collective-permute-start(bf16[256,1024]{1,0:T(8,128)(2,1)} %get-tuple-element.166), channel_id=1, source_target_pairs={{0,8},{2,10},{4,12},{6,14},{8,0},{10,2},{12,4},{14,6},{1,9},{3,11}... | collective-permute-start | bytes 1572872 | tf_op jit(solution)/shard_map/ppermute | solution.py:25
  718.5 15.9 %collective-permute-done.53.refs_3_ = bf16[256,1024]{1,0:T(8,128)(2,1)} collective-permute-done((bf16[256,1024]{1,0:T(8,128)(2,1)}, bf16[256,1024]{1,0:T(8,128)(2,1)}, u32[]{:S(2)}, u32[]{:S(2)}) %collective-permute-start.53) | collective-permute-done | bytes 524320 | tf_op jit(solution)/shard_map/ppermute | solution.py:25
  734.4 15.0 %collective-permute-start.56 = (bf16[256,1024]{1,0:T(8,128)(2,1)}, bf16[256,1024]{1,0:T(8,128)(2,1)}, u32[]{:S(2)}, u32[]{:S(2)}) collective-permute-start(bf16[256,1024]{1,0:T(8,128)(2,1)} %get-tuple-element.168), channel_id=1, source_target_pairs={{0,12},{2,14},{4,0},{6,2},{8,4},{10,6},{12,8},{14,10},{1,13},{3,15... | collective-permute-start | bytes 1572872 | tf_op jit(solution)/shard_map/ppermute | solution.py:25
  749.4 4.3 split.15
  754.3 17.8 %collective-permute-start.80 = (bf16[256,1024]{1,0:T(8,128)(2,1)}, bf16[256,1024]{1,0:T(8,128)(2,1)S(1)}, u32[]{:S(2)}, u32[]{:S(2)}) collective-permute-start(bf16[256,1024]{1,0:T(8,128)(2,1)} %get-tuple-element.196), channel_id=1, source_target_pairs={{0,4},{2,6},{4,8},{6,10},{8,12},{10,14},{12,0},{14,2},{1,5},{3,7},... | collective-permute-start | bytes 1572872 | tf_op jit(solution)/shard_map/ppermute | solution.py:25
  772.2 34.3 %collective-permute-start.82 = (bf16[256,1024]{1,0:T(8,128)(2,1)}, bf16[256,1024]{1,0:T(8,128)(2,1)}, u32[]{:S(2)}, u32[]{:S(2)}) collective-permute-start(bf16[256,1024]{1,0:T(8,128)(2,1)} %get-tuple-element.198), channel_id=1, source_target_pairs={{0,8},{2,10},{4,12},{6,14},{8,0},{10,2},{12,4},{14,6},{1,9},{3,11}... | collective-permute-start | bytes 1572872 | tf_op jit(solution)/shard_map/ppermute | solution.py:25
  814.3 12.1 %collective-permute-done.81.refs_11_ = bf16[256,1024]{1,0:T(8,128)(2,1)} collective-permute-done((bf16[256,1024]{1,0:T(8,128)(2,1)}, bf16[256,1024]{1,0:T(8,128)(2,1)}, u32[]{:S(2)}, u32[]{:S(2)}) %collective-permute-start.81) | collective-permute-done | bytes 524320 | tf_op jit(solution)/shard_map/ppermute | solution.py:25
  826.3 11.7 %collective-permute-start.84 = (bf16[256,1024]{1,0:T(8,128)(2,1)}, bf16[256,1024]{1,0:T(8,128)(2,1)S(1)}, u32[]{:S(2)}, u32[]{:S(2)}) collective-permute-start(bf16[256,1024]{1,0:T(8,128)(2,1)} %get-tuple-element.200), channel_id=1, source_target_pairs={{0,12},{2,14},{4,0},{6,2},{8,4},{10,6},{12,8},{14,10},{1,13},{3,15... | collective-permute-start | bytes 1572872 | tf_op jit(solution)/shard_map/ppermute | solution.py:25
  838.0 16.4 %collective-permute-start.85 = (bf16[256,1024]{1,0:T(8,128)(2,1)}, bf16[256,1024]{1,0:T(8,128)(2,1)}, u32[]{:S(2)}, u32[]{:S(2)}) collective-permute-start(bf16[256,1024]{1,0:T(8,128)(2,1)} %get-tuple-element.161.after_ref), channel_id=1, source_target_pairs={{0,14},{2,0},{4,2},{6,4},{8,6},{10,8},{12,10},{14,12},{1,15},{3,1}... | collective-permute-start | bytes 1572872 | tf_op jit(solution)/shard_map/ppermute | solution.py:25
  854.4 8.6 up_project.4
  865.3 5.9 down_project.4
  873.8 6.2 collective-permute-done.73.refs_2_
  881.5 37.2 %collective-permute-done.74.refs_3_ = bf16[256,1024]{1,0:T(8,128)(2,1)} collective-permute-done((bf16[256,1024]{1,0:T(8,128)(2,1)}, bf16[256,1024]{1,0:T(8,128)(2,1)}, u32[]{:S(2)}, u32[]{:S(2)}) %collective-permute-start.74) | collective-permute-done | bytes 524320 | tf_op jit(solution)/shard_map/ppermute | solution.py:25
  922.3 19.2 %collective-permute-done.76.refs_5_ = bf16[256,1024]{1,0:T(8,128)(2,1)} collective-permute-done((bf16[256,1024]{1,0:T(8,128)(2,1)}, bf16[256,1024]{1,0:T(8,128)(2,1)}, u32[]{:S(2)}, u32[]{:S(2)}) %collective-permute-start.76) | collective-permute-done | bytes 524320 | tf_op jit(solution)/shard_map/ppermute | solution.py:25
  947.2 5.1 collective-permute-start.78
  952.3 9.0 up_project.5
  961.3 5.7 down_project.5
  972.1 8.6 up_project.6
  980.7 5.7 down_project.6
  988.5 6.2 collective-permute-done.90.refs_2_
  995.0 4.6 collective-permute-done.91.refs_0_
  1014.6 9.0 up_project.7
  1023.6 5.8 down_project.7
  1029.5 17.1 %collective-permute-start.100 = (bf16[32,2048]{1,0:T(8,128)(2,1)S(1)}, bf16[32,2048]{1,0:T(8,128)(2,1)S(1)}, u32[]{:S(2)}, u32[]{:S(2)}) collective-permute-start(bf16[32,2048]{1,0:T(8,128)(2,1)S(1)} %copy-done.43), channel_id=1, source_target_pairs={{0,4},{2,6},{4,8},{6,10},{8,12},{10,14},{12,0},{14,2},{1,5},{3,7},... | collective-permute-start | bytes 393224 | tf_op jit(solution)/shard_map/ppermute | solution.py:25
  1065.6 7.4 collective-permute-done.102.refs_1_
  1078.3 13.4 %collective-permute-done.104 = f32[64,2048]{1,0:T(8,128)S(1)} collective-permute-done((f32[64,2048]{1,0:T(8,128)S(1)}, f32[64,2048]{1,0:T(8,128)S(1)}, u32[]{:S(2)}, u32[]{:S(2)}) %collective-permute-start.104) | collective-permute-done | bytes 524320 | tf_op jit(solution)/shard_map/ppermute | solution.py:25
  (351 shorter events, 234.3 us)
Async XLA Ops:
  9.2 34.7 %collective-permute-start = (bf16[1,4,128,1024]{3,2,1,0:T(8,128)(2,1)}, bf16[1,4,128,1024]{3,2,1,0:T(8,128)(2,1)S(1)}, u32[]{:S(2)}, u32[]{:S(2)}) collective-permute-start(bf16[1,4,128,1024]{3,2,1,0:T(8,128)(2,1)} %get-tuple-element.117.after_ref), channel_id=1, source_target_pairs={{0,16},{16,0},{1,17},{17,1},{2,18},{18,2},{3,19},{19,3},{4,20},{20... | collective-permute-start | bytes 3145736 | tf_op jit(solution)/shard_map/ppermute | solution.py:25
  24.2 26.8 %collective-permute-start.3 = (bf16[128,2048]{1,0:T(8,128)(2,1)}, bf16[128,2048]{1,0:T(8,128)(2,1)}, u32[]{:S(2)}, u32[]{:S(2)}) collective-permute-start(bf16[128,2048]{1,0:T(8,128)(2,1)} %convolution_convert_fusion.after_ref.refs_0_), channel_id=1, source_target_pairs={{0,4},{2,6},{4,8},{6,10},{8,12},{10,14},{12,0},{14,2},{1,5},{3,7},... | collective-permute-start | bytes 1572872 | tf_op jit(solution)/shard_map/ppermute | solution.py:25
  25.8 36.5 %collective-permute-start.4 = (bf16[128,2048]{1,0:T(8,128)(2,1)}, bf16[128,2048]{1,0:T(8,128)(2,1)}, u32[]{:S(2)}, u32[]{:S(2)}) collective-permute-start(bf16[128,2048]{1,0:T(8,128)(2,1)} %convolution_convert_fusion.after_ref.refs_0_), channel_id=1, source_target_pairs={{0,8},{2,10},{4,12},{6,14},{8,0},{10,2},{12,4},{14,6},{1,9},{3,11}... | collective-permute-start | bytes 1572872 | tf_op jit(solution)/shard_map/ppermute | solution.py:25
  28.4 58.6 %collective-permute-start.1 = (bf16[1,4,128,1024]{3,2,1,0:T(8,128)(2,1)}, bf16[1,4,128,1024]{3,2,1,0:T(8,128)(2,1)}, u32[]{:S(2)}, u32[]{:S(2)}) collective-permute-start(bf16[1,4,128,1024]{3,2,1,0:T(8,128)(2,1)} %get-tuple-element.118.after_ref), channel_id=1, source_target_pairs={{0,16},{16,0},{1,17},{17,1},{2,18},{18,2},{3,19},{19,3},{4,20},{20... | collective-permute-start | bytes 3145736 | tf_op jit(solution)/shard_map/ppermute | solution.py:25
  47.9 43.6 %collective-permute-start.2 = (bf16[4,128,1024]{2,1,0:T(8,128)(2,1)}, bf16[4,128,1024]{2,1,0:T(8,128)(2,1)}, u32[]{:S(2)}, u32[]{:S(2)}) collective-permute-start(bf16[4,128,1024]{2,1,0:T(8,128)(2,1)} %choose.12.after_ref), channel_id=1, source_target_pairs={{0,1},{1,0},{2,3},{3,2},{4,5},{5,4},{6,7},{7,6},{8,9},{9,8},{10,11... | collective-permute-start | bytes 3145736 | tf_op jit(solution)/shard_map/ppermute | solution.py:25
  49.4 145.3 %collective-permute-start.18 = (bf16[1,4,256,1024]{3,2,1,0:T(8,128)(2,1)S(1)}, bf16[1,4,256,1024]{3,2,1,0:T(8,128)(2,1)}, u32[]{:S(2)}, u32[]{:S(2)}) collective-permute-start(bf16[1,4,256,1024]{3,2,1,0:T(8,128)(2,1)S(1)} %copy-done.1), channel_id=1, source_target_pairs={{0,16},{16,0},{1,17},{17,1},{2,18},{18,2},{3,19},{19,3},{4,20},{20... | collective-permute-start | bytes 6291464 | tf_op jit(solution)/shard_map/ppermute | solution.py:25
  51.0 146.5 %collective-permute-start.26 = (bf16[1,4,256,1024]{3,2,1,0:T(8,128)(2,1)}, bf16[1,4,256,1024]{3,2,1,0:T(8,128)(2,1)}, u32[]{:S(2)}, u32[]{:S(2)}) collective-permute-start(bf16[1,4,256,1024]{3,2,1,0:T(8,128)(2,1)} %pack.13.after_ref.refs_0_), channel_id=1, source_target_pairs={{0,16},{16,0},{1,17},{17,1},{2,18},{18,2},{3,19},{19,3},{4,20},{20... | collective-permute-start | bytes 6291464 | tf_op jit(solution)/shard_map/ppermute | solution.py:25
  76.4 94.9 %collective-permute-start.6 = (bf16[1,4,128,1024]{3,2,1,0:T(8,128)(2,1)}, bf16[1,4,128,1024]{3,2,1,0:T(8,128)(2,1)S(1)}, u32[]{:S(2)}, u32[]{:S(2)}) collective-permute-start(bf16[1,4,128,1024]{3,2,1,0:T(8,128)(2,1)} %get-tuple-element.119), channel_id=1, source_target_pairs={{0,16},{16,0},{1,17},{17,1},{2,18},{18,2},{3,19},{19,3},{4,20},{20... | collective-permute-start | bytes 3145736 | tf_op jit(solution)/shard_map/ppermute | solution.py:25
  87.0 106.0 %collective-permute-start.8 = (bf16[1,4,128,1024]{3,2,1,0:T(8,128)(2,1)}, bf16[1,4,128,1024]{3,2,1,0:T(8,128)(2,1)}, u32[]{:S(2)}, u32[]{:S(2)}) collective-permute-start(bf16[1,4,128,1024]{3,2,1,0:T(8,128)(2,1)} %get-tuple-element.121.after_ref), channel_id=1, source_target_pairs={{0,16},{16,0},{1,17},{17,1},{2,18},{18,2},{3,19},{19,3},{4,20},{20... | collective-permute-start | bytes 3145736 | tf_op jit(solution)/shard_map/ppermute | solution.py:25
  91.5 103.3 %collective-permute-start.7 = (bf16[4,128,1024]{2,1,0:T(8,128)(2,1)}, bf16[4,128,1024]{2,1,0:T(8,128)(2,1)}, u32[]{:S(2)}, u32[]{:S(2)}) collective-permute-start(bf16[4,128,1024]{2,1,0:T(8,128)(2,1)} %choose.13.after_ref), channel_id=1, source_target_pairs={{0,1},{1,0},{2,3},{3,2},{4,5},{5,4},{6,7},{7,6},{8,9},{9,8},{10,11... | collective-permute-start | bytes 3145736 | tf_op jit(solution)/shard_map/ppermute | solution.py:25
  171.2 28.5 %collective-permute-start.10 = (bf16[128,1024]{1,0:T(8,128)(2,1)}, bf16[128,1024]{1,0:T(8,128)(2,1)}, u32[]{:S(2)}, u32[]{:S(2)}) collective-permute-start(bf16[128,1024]{1,0:T(8,128)(2,1)} %get-tuple-element.130), channel_id=1, source_target_pairs={{0,2},{2,4},{4,6},{6,8},{8,10},{10,12},{12,14},{14,0},{1,3},{3,5},... | collective-permute-start | bytes 786440 | tf_op jit(solution)/shard_map/ppermute | solution.py:25
  193.0 27.0 %collective-permute-start.11 = (bf16[128,1024]{1,0:T(8,128)(2,1)}, bf16[128,1024]{1,0:T(8,128)(2,1)}, u32[]{:S(2)}, u32[]{:S(2)}) collective-permute-start(bf16[128,1024]{1,0:T(8,128)(2,1)} %get-tuple-element.131), channel_id=1, source_target_pairs={{0,4},{2,6},{4,8},{6,10},{8,12},{10,14},{12,0},{14,2},{1,5},{3,7},... | collective-permute-start | bytes 786440 | tf_op jit(solution)/shard_map/ppermute | solution.py:25
  194.8 27.4 %collective-permute-start.12 = (bf16[128,1024]{1,0:T(8,128)(2,1)}, bf16[128,1024]{1,0:T(8,128)(2,1)}, u32[]{:S(2)}, u32[]{:S(2)}) collective-permute-start(bf16[128,1024]{1,0:T(8,128)(2,1)} %get-tuple-element.132), channel_id=1, source_target_pairs={{0,6},{2,8},{4,10},{6,12},{8,14},{10,0},{12,2},{14,4},{1,7},{3,9},... | collective-permute-start | bytes 786440 | tf_op jit(solution)/shard_map/ppermute | solution.py:25
  194.8 27.5 %collective-permute-start.13 = (bf16[128,1024]{1,0:T(8,128)(2,1)}, bf16[128,1024]{1,0:T(8,128)(2,1)}, u32[]{:S(2)}, u32[]{:S(2)}) collective-permute-start(bf16[128,1024]{1,0:T(8,128)(2,1)} %get-tuple-element.133), channel_id=1, source_target_pairs={{0,8},{2,10},{4,12},{6,14},{8,0},{10,2},{12,4},{14,6},{1,9},{3,11}... | collective-permute-start | bytes 786440 | tf_op jit(solution)/shard_map/ppermute | solution.py:25
  197.4 26.4 %collective-permute-start.14 = (bf16[128,1024]{1,0:T(8,128)(2,1)}, bf16[128,1024]{1,0:T(8,128)(2,1)}, u32[]{:S(2)}, u32[]{:S(2)}) collective-permute-start(bf16[128,1024]{1,0:T(8,128)(2,1)} %get-tuple-element.134), channel_id=1, source_target_pairs={{0,10},{2,12},{4,14},{6,0},{8,2},{10,4},{12,6},{14,8},{1,11},{3,13... | collective-permute-start | bytes 786440 | tf_op jit(solution)/shard_map/ppermute | solution.py:25
  222.3 90.5 %collective-permute-start.35 = (bf16[1,4,256,1024]{3,2,1,0:T(8,128)(2,1)}, bf16[1,4,256,1024]{3,2,1,0:T(8,128)(2,1)}, u32[]{:S(2)}, u32[]{:S(2)}) collective-permute-start(bf16[1,4,256,1024]{3,2,1,0:T(8,128)(2,1)} %pack.14.after_ref.refs_0_), channel_id=1, source_target_pairs={{0,16},{16,0},{1,17},{17,1},{2,18},{18,2},{3,19},{19,3},{4,20},{20... | collective-permute-start | bytes 6291464 | tf_op jit(solution)/shard_map/ppermute | solution.py:25
  223.8 99.1 %collective-permute-start.44 = (bf16[1,4,256,1024]{3,2,1,0:T(8,128)(2,1)}, bf16[1,4,256,1024]{3,2,1,0:T(8,128)(2,1)}, u32[]{:S(2)}, u32[]{:S(2)}) collective-permute-start(bf16[1,4,256,1024]{3,2,1,0:T(8,128)(2,1)} %pack.15.after_ref.refs_0_), channel_id=1, source_target_pairs={{0,16},{16,0},{1,17},{17,1},{2,18},{18,2},{3,19},{19,3},{4,20},{20... | collective-permute-start | bytes 6291464 | tf_op jit(solution)/shard_map/ppermute | solution.py:25
  224.3 128.3 %collective-permute-start.46 = (bf16[1,1024,1024]{2,1,0:T(8,128)(2,1)S(1)}, bf16[1,1024,1024]{2,1,0:T(8,128)(2,1)}, u32[]{:S(2)}, u32[]{:S(2)}) collective-permute-start(bf16[1,1024,1024]{2,1,0:T(8,128)(2,1)S(1)} %copy-done.2), channel_id=1, source_target_pairs={{0,16},{16,0},{1,17},{17,1},{2,18},{18,2},{3,19},{19,3},{4,20},{20... | collective-permute-start | bytes 6291464 | tf_op jit(solution)/shard_map/ppermute | solution.py:25
  242.7 24.8 %collective-permute-start.21 = (bf16[128,1024]{1,0:T(8,128)(2,1)}, bf16[128,1024]{1,0:T(8,128)(2,1)S(1)}, u32[]{:S(2)}, u32[]{:S(2)}) collective-permute-start(bf16[128,1024]{1,0:T(8,128)(2,1)} %get-tuple-element.140), channel_id=1, source_target_pairs={{0,6},{2,8},{4,10},{6,12},{8,14},{10,0},{12,2},{14,4},{1,7},{3,9},... | collective-permute-start | bytes 786440 | tf_op jit(solution)/shard_map/ppermute | solution.py:25
  285.7 26.3 %collective-permute-start.17 = (bf16[4,128,1024]{2,1,0:T(8,128)(2,1)}, bf16[4,128,1024]{2,1,0:T(8,128)(2,1)}, u32[]{:S(2)}, u32[]{:S(2)}) collective-permute-start(bf16[4,128,1024]{2,1,0:T(8,128)(2,1)} %choose.15.after_ref), channel_id=1, source_target_pairs={{0,1},{1,0},{2,3},{3,2},{4,5},{5,4},{6,7},{7,6},{8,9},{9,8},{10,11... | collective-permute-start | bytes 3145736 | tf_op jit(solution)/shard_map/ppermute | solution.py:25
  308.6 45.5 %collective-permute-start.28 = (bf16[128,1024]{1,0:T(8,128)(2,1)}, bf16[128,1024]{1,0:T(8,128)(2,1)S(1)}, u32[]{:S(2)}, u32[]{:S(2)}) collective-permute-start(bf16[128,1024]{1,0:T(8,128)(2,1)} %get-tuple-element.146), channel_id=1, source_target_pairs={{0,2},{2,4},{4,6},{6,8},{8,10},{10,12},{12,14},{14,0},{1,3},{3,5},... | collective-permute-start | bytes 786440 | tf_op jit(solution)/shard_map/ppermute | solution.py:25
  312.1 55.0 %collective-permute-start.29 = (bf16[128,1024]{1,0:T(8,128)(2,1)}, bf16[128,1024]{1,0:T(8,128)(2,1)S(1)}, u32[]{:S(2)}, u32[]{:S(2)}) collective-permute-start(bf16[128,1024]{1,0:T(8,128)(2,1)} %get-tuple-element.147), channel_id=1, source_target_pairs={{0,4},{2,6},{4,8},{6,10},{8,12},{10,14},{12,0},{14,2},{1,5},{3,7},... | collective-permute-start | bytes 786440 | tf_op jit(solution)/shard_map/ppermute | solution.py:25
  312.8 154.6 %collective-permute-start.48 = (bf16[1,1024,1024]{2,1,0:T(8,128)(2,1)}, bf16[1,1024,1024]{2,1,0:T(8,128)(2,1)}, u32[]{:S(2)}, u32[]{:S(2)}) collective-permute-start(bf16[1,1024,1024]{2,1,0:T(8,128)(2,1)} %cast.5.after_ref.refs_0_), channel_id=1, source_target_pairs={{0,16},{16,0},{1,17},{17,1},{2,18},{18,2},{3,19},{19,3},{4,20},{20... | collective-permute-start | bytes 6291464 | tf_op jit(solution)/shard_map/ppermute | solution.py:25
  322.9 146.1 %collective-permute-start.49 = (bf16[1,1024,1024]{2,1,0:T(8,128)(2,1)}, bf16[1,1024,1024]{2,1,0:T(8,128)(2,1)}, u32[]{:S(2)}, u32[]{:S(2)}) collective-permute-start(bf16[1,1024,1024]{2,1,0:T(8,128)(2,1)} %cast.6.after_ref.refs_0_), channel_id=1, source_target_pairs={{0,16},{16,0},{1,17},{17,1},{2,18},{18,2},{3,19},{19,3},{4,20},{20... | collective-permute-start | bytes 6291464 | tf_op jit(solution)/shard_map/ppermute | solution.py:25
  352.7 116.9 %collective-permute-start.27 = (bf16[4,256,1024]{2,1,0:T(8,128)(2,1)}, bf16[4,256,1024]{2,1,0:T(8,128)(2,1)}, u32[]{:S(2)}, u32[]{:S(2)}) collective-permute-start(bf16[4,256,1024]{2,1,0:T(8,128)(2,1)} %choose.16.after_ref), channel_id=1, source_target_pairs={{0,1},{1,0},{2,3},{3,2},{4,5},{5,4},{6,7},{7,6},{8,9},{9,8},{10,11... | collective-permute-start | bytes 6291464 | tf_op jit(solution)/shard_map/ppermute | solution.py:25
  375.0 28.4 %collective-permute-start.32 = (bf16[128,1024]{1,0:T(8,128)(2,1)}, bf16[128,1024]{1,0:T(8,128)(2,1)S(1)}, u32[]{:S(2)}, u32[]{:S(2)}) collective-permute-start(bf16[128,1024]{1,0:T(8,128)(2,1)} %get-tuple-element.150), channel_id=1, source_target_pairs={{0,10},{2,12},{4,14},{6,0},{8,2},{10,4},{12,6},{14,8},{1,11},{3,13... | collective-permute-start | bytes 786440 | tf_op jit(solution)/shard_map/ppermute | solution.py:25
  417.4 24.6 %collective-permute-start.39 = (bf16[128,1024]{1,0:T(8,128)(2,1)}, bf16[128,1024]{1,0:T(8,128)(2,1)}, u32[]{:S(2)}, u32[]{:S(2)}) collective-permute-start(bf16[128,1024]{1,0:T(8,128)(2,1)} %get-tuple-element.156), channel_id=1, source_target_pairs={{0,6},{2,8},{4,10},{6,12},{8,14},{10,0},{12,2},{14,4},{1,7},{3,9},... | collective-permute-start | bytes 786440 | tf_op jit(solution)/shard_map/ppermute | solution.py:25
  448.3 47.8 %collective-permute-start.36 = (bf16[4,256,1024]{2,1,0:T(8,128)(2,1)}, bf16[4,256,1024]{2,1,0:T(8,128)(2,1)}, u32[]{:S(2)}, u32[]{:S(2)}) collective-permute-start(bf16[4,256,1024]{2,1,0:T(8,128)(2,1)} %choose.17.after_ref), channel_id=1, source_target_pairs={{0,1},{1,0},{2,3},{3,2},{4,5},{5,4},{6,7},{7,6},{8,9},{9,8},{10,11... | collective-permute-start | bytes 6291464 | tf_op jit(solution)/shard_map/ppermute | solution.py:25
  467.4 33.5 %collective-permute-start.50 = (bf16[4,128,2048]{2,1,0:T(8,128)(2,1)S(1)}, bf16[4,128,2048]{2,1,0:T(8,128)(2,1)}, u32[]{:S(2)}, u32[]{:S(2)}) collective-permute-start(bf16[4,128,2048]{2,1,0:T(8,128)(2,1)S(1)} %copy-done), channel_id=1, source_target_pairs={{0,2},{2,0},{4,6},{6,4},{8,10},{10,8},{12,14},{14,12},{1,3},{3,1},... | collective-permute-start | bytes 6291464 | tf_op jit(solution)/shard_map/ppermute | solution.py:488
  467.4 48.9 %collective-permute-start.67 = (bf16[1,1024,1024]{2,1,0:T(8,128)(2,1)}, bf16[1,1024,1024]{2,1,0:T(8,128)(2,1)}, u32[]{:S(2)}, u32[]{:S(2)}) collective-permute-start(bf16[1,1024,1024]{2,1,0:T(8,128)(2,1)} %cast.7.after_ref.refs_0_), channel_id=1, source_target_pairs={{0,16},{16,0},{1,17},{17,1},{2,18},{18,2},{3,19},{19,3},{4,20},{20... | collective-permute-start | bytes 6291464 | tf_op jit(solution)/shard_map/ppermute | solution.py:25
  469.0 92.2 %collective-permute-start.69 = (bf16[8,128,1024]{2,1,0:T(8,128)(2,1)}, bf16[8,128,1024]{2,1,0:T(8,128)(2,1)}, u32[]{:S(2)}, u32[]{:S(2)}) collective-permute-start(bf16[8,128,1024]{2,1,0:T(8,128)(2,1)} %stack.23.after_ref.refs_2_), channel_id=1, source_target_pairs={{0,16},{16,0},{1,17},{17,1},{2,18},{18,2},{3,19},{19,3},{4,20},{20... | collective-permute-start | bytes 6291464 | tf_op jit(solution)/shard_map/ppermute | solution.py:25
  469.5 136.1 %collective-permute-start.68 = (bf16[8,128,1024]{2,1,0:T(8,128)(2,1)}, bf16[8,128,1024]{2,1,0:T(8,128)(2,1)}, u32[]{:S(2)}, u32[]{:S(2)}) collective-permute-start(bf16[8,128,1024]{2,1,0:T(8,128)(2,1)} %stack.22.after_ref.refs_0_), channel_id=1, source_target_pairs={{0,16},{16,0},{1,17},{17,1},{2,18},{18,2},{3,19},{19,3},{4,20},{20... | collective-permute-start | bytes 6291464 | tf_op jit(solution)/shard_map/ppermute | solution.py:25
  496.1 180.1 %collective-permute-start.45 = (bf16[4,256,1024]{2,1,0:T(8,128)(2,1)}, bf16[4,256,1024]{2,1,0:T(8,128)(2,1)}, u32[]{:S(2)}, u32[]{:S(2)}) collective-permute-start(bf16[4,256,1024]{2,1,0:T(8,128)(2,1)} %choose.18.after_ref), channel_id=1, source_target_pairs={{0,1},{1,0},{2,3},{3,2},{4,5},{5,4},{6,7},{7,6},{8,9},{9,8},{10,11... | collective-permute-start | bytes 6291464 | tf_op jit(solution)/shard_map/ppermute | solution.py:25
  500.9 104.8 %collective-permute-start.58 = (bf16[256,1024]{1,0:T(8,128)(2,1)}, bf16[256,1024]{1,0:T(8,128)(2,1)S(1)}, u32[]{:S(2)}, u32[]{:S(2)}) collective-permute-start(bf16[256,1024]{1,0:T(8,128)(2,1)} %get-tuple-element.170), channel_id=1, source_target_pairs={{0,2},{2,4},{4,6},{6,8},{8,10},{10,12},{12,14},{14,0},{1,3},{3,5},... | collective-permute-start | bytes 1572872 | tf_op jit(solution)/shard_map/ppermute | solution.py:25
  516.3 233.1 %collective-permute-start.47 = (bf16[4,256,1024]{2,1,0:T(8,128)(2,1)}, bf16[4,256,1024]{2,1,0:T(8,128)(2,1)}, u32[]{:S(2)}, u32[]{:S(2)}) collective-permute-start(bf16[4,256,1024]{2,1,0:T(8,128)(2,1)} %choose.19.after_ref), channel_id=1, source_target_pairs={{0,1},{1,0},{2,3},{3,2},{4,5},{5,4},{6,7},{7,6},{8,9},{9,8},{10,11... | collective-permute-start | bytes 6291464 | tf_op jit(solution)/shard_map/ppermute | solution.py:25
  561.2 47.4 %collective-permute-start.59 = (bf16[256,1024]{1,0:T(8,128)(2,1)}, bf16[256,1024]{1,0:T(8,128)(2,1)}, u32[]{:S(2)}, u32[]{:S(2)}) collective-permute-start(bf16[256,1024]{1,0:T(8,128)(2,1)} %get-tuple-element.171), channel_id=1, source_target_pairs={{0,4},{2,6},{4,8},{6,10},{8,12},{10,14},{12,0},{14,2},{1,5},{3,7},... | collective-permute-start | bytes 1572872 | tf_op jit(solution)/shard_map/ppermute | solution.py:25
  605.7 43.0 %collective-permute-start.60 = (bf16[256,1024]{1,0:T(8,128)(2,1)S(1)}, bf16[256,1024]{1,0:T(8,128)(2,1)}, u32[]{:S(2)}, u32[]{:S(2)}) collective-permute-start(bf16[256,1024]{1,0:T(8,128)(2,1)S(1)} %copy-done.59), channel_id=1, source_target_pairs={{0,6},{2,8},{4,10},{6,12},{8,14},{10,0},{12,2},{14,4},{1,7},{3,9},... | collective-permute-start | bytes 1572872 | tf_op jit(solution)/shard_map/ppermute | solution.py:25
  605.7 51.9 %collective-permute-start.61 = (bf16[256,1024]{1,0:T(8,128)(2,1)S(1)}, bf16[256,1024]{1,0:T(8,128)(2,1)}, u32[]{:S(2)}, u32[]{:S(2)}) collective-permute-start(bf16[256,1024]{1,0:T(8,128)(2,1)S(1)} %copy-done.58), channel_id=1, source_target_pairs={{0,8},{2,10},{4,12},{6,14},{8,0},{10,2},{12,4},{14,6},{1,9},{3,11}... | collective-permute-start | bytes 1572872 | tf_op jit(solution)/shard_map/ppermute | solution.py:25
  608.7 65.2 %collective-permute-start.62 = (bf16[256,1024]{1,0:T(8,128)(2,1)S(1)}, bf16[256,1024]{1,0:T(8,128)(2,1)}, u32[]{:S(2)}, u32[]{:S(2)}) collective-permute-start(bf16[256,1024]{1,0:T(8,128)(2,1)S(1)} %copy-done.57), channel_id=1, source_target_pairs={{0,10},{2,12},{4,14},{6,0},{8,2},{10,4},{12,6},{14,8},{1,11},{3,13... | collective-permute-start | bytes 1572872 | tf_op jit(solution)/shard_map/ppermute | solution.py:25
  648.7 25.3 %collective-permute-start.63 = (bf16[256,1024]{1,0:T(8,128)(2,1)S(1)}, bf16[256,1024]{1,0:T(8,128)(2,1)}, u32[]{:S(2)}, u32[]{:S(2)}) collective-permute-start(bf16[256,1024]{1,0:T(8,128)(2,1)S(1)} %copy-done.56), channel_id=1, source_target_pairs={{0,12},{2,14},{4,0},{6,2},{8,4},{10,6},{12,8},{14,10},{1,13},{3,15... | collective-permute-start | bytes 1572872 | tf_op jit(solution)/shard_map/ppermute | solution.py:25
  657.5 30.0 %collective-permute-start.64 = (bf16[256,1024]{1,0:T(8,128)(2,1)S(1)}, bf16[256,1024]{1,0:T(8,128)(2,1)}, u32[]{:S(2)}, u32[]{:S(2)}) collective-permute-start(bf16[256,1024]{1,0:T(8,128)(2,1)S(1)} %copy-done.17), channel_id=1, source_target_pairs={{0,14},{2,0},{4,2},{6,4},{8,6},{10,8},{12,10},{14,12},{1,15},{3,1}... | collective-permute-start | bytes 1572872 | tf_op jit(solution)/shard_map/ppermute | solution.py:25
  673.9 44.6 %collective-permute-start.52 = (bf16[256,1024]{1,0:T(8,128)(2,1)}, bf16[256,1024]{1,0:T(8,128)(2,1)S(1)}, u32[]{:S(2)}, u32[]{:S(2)}) collective-permute-start(bf16[256,1024]{1,0:T(8,128)(2,1)} %get-tuple-element.164), channel_id=1, source_target_pairs={{0,4},{2,6},{4,8},{6,10},{8,12},{10,14},{12,0},{14,2},{1,5},{3,7},... | collective-permute-start | bytes 1572872 | tf_op jit(solution)/shard_map/ppermute | solution.py:25
  676.1 58.3 %collective-permute-start.53 = (bf16[256,1024]{1,0:T(8,128)(2,1)}, bf16[256,1024]{1,0:T(8,128)(2,1)}, u32[]{:S(2)}, u32[]{:S(2)}) collective-permute-start(bf16[256,1024]{1,0:T(8,128)(2,1)} %get-tuple-element.165), channel_id=1, source_target_pairs={{0,6},{2,8},{4,10},{6,12},{8,14},{10,0},{12,2},{14,4},{1,7},{3,9},... | collective-permute-start | bytes 1572872 | tf_op jit(solution)/shard_map/ppermute | solution.py:25
  687.5 176.5 %collective-permute-start.65 = (bf16[1024,1024]{1,0:T(8,128)(2,1)}, bf16[1024,1024]{1,0:T(8,128)(2,1)S(1)}, u32[]{:S(2)}, u32[]{:S(2)}) collective-permute-start(bf16[1024,1024]{1,0:T(8,128)(2,1)} %choose.20.after_ref), channel_id=1, source_target_pairs={{0,1},{1,0},{2,3},{3,2},{4,5},{5,4},{6,7},{7,6},{8,9},{9,8},{10,11... | collective-permute-start | bytes 6291464 | tf_op jit(solution)/shard_map/ppermute | solution.py:25
  690.5 63.2 %collective-permute-start.54 = (bf16[256,1024]{1,0:T(8,128)(2,1)}, bf16[256,1024]{1,0:T(8,128)(2,1)}, u32[]{:S(2)}, u32[]{:S(2)}) collective-permute-start(bf16[256,1024]{1,0:T(8,128)(2,1)} %get-tuple-element.166), channel_id=1, source_target_pairs={{0,8},{2,10},{4,12},{6,14},{8,0},{10,2},{12,4},{14,6},{1,9},{3,11}... | collective-permute-start | bytes 1572872 | tf_op jit(solution)/shard_map/ppermute | solution.py:25
  718.5 35.8 %collective-permute-start.55 = (bf16[256,1024]{1,0:T(8,128)(2,1)}, bf16[256,1024]{1,0:T(8,128)(2,1)}, u32[]{:S(2)}, u32[]{:S(2)}) collective-permute-start(bf16[256,1024]{1,0:T(8,128)(2,1)} %get-tuple-element.167), channel_id=1, source_target_pairs={{0,10},{2,12},{4,14},{6,0},{8,2},{10,4},{12,6},{14,8},{1,11},{3,13... | collective-permute-start | bytes 1572872 | tf_op jit(solution)/shard_map/ppermute | solution.py:25
  734.4 37.7 %collective-permute-start.56 = (bf16[256,1024]{1,0:T(8,128)(2,1)}, bf16[256,1024]{1,0:T(8,128)(2,1)}, u32[]{:S(2)}, u32[]{:S(2)}) collective-permute-start(bf16[256,1024]{1,0:T(8,128)(2,1)} %get-tuple-element.168), channel_id=1, source_target_pairs={{0,12},{2,14},{4,0},{6,2},{8,4},{10,6},{12,8},{14,10},{1,13},{3,15... | collective-permute-start | bytes 1572872 | tf_op jit(solution)/shard_map/ppermute | solution.py:25
  753.8 52.7 %collective-permute-start.79 = (bf16[256,1024]{1,0:T(8,128)(2,1)}, bf16[256,1024]{1,0:T(8,128)(2,1)S(1)}, u32[]{:S(2)}, u32[]{:S(2)}) collective-permute-start(bf16[256,1024]{1,0:T(8,128)(2,1)} %get-tuple-element.195), channel_id=1, source_target_pairs={{0,2},{2,4},{4,6},{6,8},{8,10},{10,12},{12,14},{14,0},{1,3},{3,5},... | collective-permute-start | bytes 1572872 | tf_op jit(solution)/shard_map/ppermute | solution.py:25
  754.3 59.3 %collective-permute-start.80 = (bf16[256,1024]{1,0:T(8,128)(2,1)}, bf16[256,1024]{1,0:T(8,128)(2,1)S(1)}, u32[]{:S(2)}, u32[]{:S(2)}) collective-permute-start(bf16[256,1024]{1,0:T(8,128)(2,1)} %get-tuple-element.196), channel_id=1, source_target_pairs={{0,4},{2,6},{4,8},{6,10},{8,12},{10,14},{12,0},{14,2},{1,5},{3,7},... | collective-permute-start | bytes 1572872 | tf_op jit(solution)/shard_map/ppermute | solution.py:25
  772.1 54.2 %collective-permute-start.81 = (bf16[256,1024]{1,0:T(8,128)(2,1)}, bf16[256,1024]{1,0:T(8,128)(2,1)}, u32[]{:S(2)}, u32[]{:S(2)}) collective-permute-start(bf16[256,1024]{1,0:T(8,128)(2,1)} %get-tuple-element.197), channel_id=1, source_target_pairs={{0,6},{2,8},{4,10},{6,12},{8,14},{10,0},{12,2},{14,4},{1,7},{3,9},... | collective-permute-start | bytes 1572872 | tf_op jit(solution)/shard_map/ppermute | solution.py:25
  772.2 65.9 %collective-permute-start.82 = (bf16[256,1024]{1,0:T(8,128)(2,1)}, bf16[256,1024]{1,0:T(8,128)(2,1)}, u32[]{:S(2)}, u32[]{:S(2)}) collective-permute-start(bf16[256,1024]{1,0:T(8,128)(2,1)} %get-tuple-element.198), channel_id=1, source_target_pairs={{0,8},{2,10},{4,12},{6,14},{8,0},{10,2},{12,4},{14,6},{1,9},{3,11}... | collective-permute-start | bytes 1572872 | tf_op jit(solution)/shard_map/ppermute | solution.py:25
  806.5 47.9 %collective-permute-start.83 = (bf16[256,1024]{1,0:T(8,128)(2,1)}, bf16[256,1024]{1,0:T(8,128)(2,1)}, u32[]{:S(2)}, u32[]{:S(2)}) collective-permute-start(bf16[256,1024]{1,0:T(8,128)(2,1)} %get-tuple-element.199), channel_id=1, source_target_pairs={{0,10},{2,12},{4,14},{6,0},{8,2},{10,4},{12,6},{14,8},{1,11},{3,13... | collective-permute-start | bytes 1572872 | tf_op jit(solution)/shard_map/ppermute | solution.py:25
  813.7 133.6 %collective-permute-start.70 = (bf16[1024,1024]{1,0:T(8,128)(2,1)}, bf16[1024,1024]{1,0:T(8,128)(2,1)}, u32[]{:S(2)}, u32[]{:S(2)}) collective-permute-start(bf16[1024,1024]{1,0:T(8,128)(2,1)} %choose.22.after_ref), channel_id=1, source_target_pairs={{0,1},{1,0},{2,3},{3,2},{4,5},{5,4},{6,7},{7,6},{8,9},{9,8},{10,11... | collective-permute-start | bytes 6291464 | tf_op jit(solution)/shard_map/ppermute | solution.py:25
  826.3 36.7 %collective-permute-start.84 = (bf16[256,1024]{1,0:T(8,128)(2,1)}, bf16[256,1024]{1,0:T(8,128)(2,1)S(1)}, u32[]{:S(2)}, u32[]{:S(2)}) collective-permute-start(bf16[256,1024]{1,0:T(8,128)(2,1)} %get-tuple-element.200), channel_id=1, source_target_pairs={{0,12},{2,14},{4,0},{6,2},{8,4},{10,6},{12,8},{14,10},{1,13},{3,15... | collective-permute-start | bytes 1572872 | tf_op jit(solution)/shard_map/ppermute | solution.py:25
  838.0 33.2 %collective-permute-start.85 = (bf16[256,1024]{1,0:T(8,128)(2,1)}, bf16[256,1024]{1,0:T(8,128)(2,1)}, u32[]{:S(2)}, u32[]{:S(2)}) collective-permute-start(bf16[256,1024]{1,0:T(8,128)(2,1)} %get-tuple-element.161.after_ref), channel_id=1, source_target_pairs={{0,14},{2,0},{4,2},{6,4},{8,6},{10,8},{12,10},{14,12},{1,15},{3,1}... | collective-permute-start | bytes 1572872 | tf_op jit(solution)/shard_map/ppermute | solution.py:25
  864.0 54.7 %collective-permute-start.74 = (bf16[256,1024]{1,0:T(8,128)(2,1)}, bf16[256,1024]{1,0:T(8,128)(2,1)}, u32[]{:S(2)}, u32[]{:S(2)}) collective-permute-start(bf16[256,1024]{1,0:T(8,128)(2,1)} %get-tuple-element.190), channel_id=1, source_target_pairs={{0,6},{2,8},{4,10},{6,12},{8,14},{10,0},{12,2},{14,4},{1,7},{3,9},... | collective-permute-start | bytes 1572872 | tf_op jit(solution)/shard_map/ppermute | solution.py:25
  871.2 47.5 %collective-permute-start.66 = (bf16[128,2048]{1,0:T(8,128)(2,1)}, bf16[128,2048]{1,0:T(8,128)(2,1)}, u32[]{:S(2)}, u32[]{:S(2)}) collective-permute-start(bf16[128,2048]{1,0:T(8,128)(2,1)} %get-tuple-element.177.after_ref), channel_id=1, source_target_pairs={{0,2},{2,0},{4,6},{6,4},{8,10},{10,8},{12,14},{14,12},{1,3},{3,1},... | collective-permute-start | bytes 1572872 | tf_op jit(solution)/shard_map/ppermute | solution.py:488
  873.3 93.8 %collective-permute-start.86 = (bf16[1024,1024]{1,0:T(8,128)(2,1)}, bf16[1024,1024]{1,0:T(8,128)(2,1)}, u32[]{:S(2)}, u32[]{:S(2)}) collective-permute-start(bf16[1024,1024]{1,0:T(8,128)(2,1)} %choose.21.after_ref), channel_id=1, source_target_pairs={{0,1},{1,0},{2,3},{3,2},{4,5},{5,4},{6,7},{7,6},{8,9},{9,8},{10,11... | collective-permute-start | bytes 6291464 | tf_op jit(solution)/shard_map/ppermute | solution.py:25
  880.0 40.8 %collective-permute-start.75 = (bf16[256,1024]{1,0:T(8,128)(2,1)}, bf16[256,1024]{1,0:T(8,128)(2,1)}, u32[]{:S(2)}, u32[]{:S(2)}) collective-permute-start(bf16[256,1024]{1,0:T(8,128)(2,1)} %get-tuple-element.191), channel_id=1, source_target_pairs={{0,8},{2,10},{4,12},{6,14},{8,0},{10,2},{12,4},{14,6},{1,9},{3,11}... | collective-permute-start | bytes 1572872 | tf_op jit(solution)/shard_map/ppermute | solution.py:25
  918.7 27.9 %collective-permute-start.77 = (bf16[256,1024]{1,0:T(8,128)(2,1)}, bf16[256,1024]{1,0:T(8,128)(2,1)}, u32[]{:S(2)}, u32[]{:S(2)}) collective-permute-start(bf16[256,1024]{1,0:T(8,128)(2,1)} %get-tuple-element.193), channel_id=1, source_target_pairs={{0,12},{2,14},{4,0},{6,2},{8,4},{10,6},{12,8},{14,10},{1,13},{3,15... | collective-permute-start | bytes 1572872 | tf_op jit(solution)/shard_map/ppermute | solution.py:25
  920.8 93.8 %collective-permute-start.95 = (bf16[8,128,1024]{2,1,0:T(8,128)(2,1)}, bf16[8,128,1024]{2,1,0:T(8,128)(2,1)}, u32[]{:S(2)}, u32[]{:S(2)}) collective-permute-start(bf16[8,128,1024]{2,1,0:T(8,128)(2,1)} %stack.25.after_ref.refs_2_), channel_id=1, source_target_pairs={{0,16},{16,0},{1,17},{17,1},{2,18},{18,2},{3,19},{19,3},{4,20},{20... | collective-permute-start | bytes 6291464 | tf_op jit(solution)/shard_map/ppermute | solution.py:25
  941.5 73.1 %collective-permute-start.94 = (bf16[8,128,1024]{2,1,0:T(8,128)(2,1)S(1)}, bf16[8,128,1024]{2,1,0:T(8,128)(2,1)}, u32[]{:S(2)}, u32[]{:S(2)}) collective-permute-start(bf16[8,128,1024]{2,1,0:T(8,128)(2,1)S(1)} %copy-done.3), channel_id=1, source_target_pairs={{0,16},{16,0},{1,17},{17,1},{2,18},{18,2},{3,19},{19,3},{4,20},{20... | collective-permute-start | bytes 6291464 | tf_op jit(solution)/shard_map/ppermute | solution.py:25
  946.6 76.9 %collective-permute-start.96 = (bf16[1024,1024]{1,0:T(8,128)(2,1)}, bf16[1024,1024]{1,0:T(8,128)(2,1)}, u32[]{:S(2)}, u32[]{:S(2)}) collective-permute-start(bf16[1024,1024]{1,0:T(8,128)(2,1)} %choose.23.after_ref), channel_id=1, source_target_pairs={{0,1},{1,0},{2,3},{3,2},{4,5},{5,4},{6,7},{7,6},{8,9},{9,8},{10,11... | collective-permute-start | bytes 6291464 | tf_op jit(solution)/shard_map/ppermute | solution.py:25
  1029.5 26.8 %collective-permute-start.100 = (bf16[32,2048]{1,0:T(8,128)(2,1)S(1)}, bf16[32,2048]{1,0:T(8,128)(2,1)S(1)}, u32[]{:S(2)}, u32[]{:S(2)}) collective-permute-start(bf16[32,2048]{1,0:T(8,128)(2,1)S(1)} %copy-done.43), channel_id=1, source_target_pairs={{0,4},{2,6},{4,8},{6,10},{8,12},{10,14},{12,0},{14,2},{1,5},{3,7},... | collective-permute-start | bytes 393224 | tf_op jit(solution)/shard_map/ppermute | solution.py:25
  (105 other events, 2533.2 us)
